TPU v7x, 32 devices: a whole 2x2x4 slice. The times are simulated.
32 devices in a mesh: sp: 8 (over z, y), tp: 4 (over x, core).
Axes of the slice: x: 2, y: 2, z: 4, core: 2. Of those that a mesh axis runs over, the one named last changes fastest.
Arguments:
- tokens: bfloat16 [2048, 4096], P('sp'), may hold values from -6 to 6
- norm_gain: float32 [4096], replicated, may hold values from 0.1 to 1.9
- w_query: bfloat16 [4096, 512], P('sp', 'tp'), may hold values from -0.09375 to 0.09375
- w_key: bfloat16 [4096, 512], P('sp', 'tp'), may hold values from -0.09375 to 0.09375
- w_value: bfloat16 [4096, 1024], P('sp', 'tp'), may hold values from -0.09375 to 0.09375
- w_gates: bfloat16 [4096, 2, 2, 4], P(None, None, None, 'tp'), may hold values from -0.09375 to 0.09375
- input_bias: float32 [2, 4], P(None, 'tp'), may hold values from -2 to 90
- forget_bias: float32 [2, 4], P(None, 'tp'), as said below
- decay_shift: float32 [2, 2048, 4], P(None, 'sp', 'tp'), may hold values from -2.5 to 0
- head_gain: float32 [1024], P('tp'), may hold values from 0.1 to 1.9
- w_conv_b: bfloat16 [4096, 1024], P('sp', 'tp'), may hold values from -0.09375 to 0.09375
- w_conv_c: bfloat16 [4096, 1024], P('sp', 'tp'), may hold values from -0.09375 to 0.09375
- w_conv_in: bfloat16 [4096, 1024], P('sp', 'tp'), may hold values from -0.09375 to 0.09375
- conv_taps: bfloat16 [3, 1024], P(None, 'tp'), may hold values from -3.5 to 3.5
- w_out: bfloat16 [2048, 4096], P('sp', 'tp'), may hold values from -0.125 to 0.125
Outputs:
- mixed_out: bfloat16 [2048, 4096], P('sp', 'tp')
Inputs may be any that keep to these rules, and one draw needn't show every extreme that they name: `forget_bias`: at most the natural logarithm of 2048 plus 2.
All inputs are finite; a program needn't handle non-finite values.
Results may differ from a plain program's by a relative error of at most 0.02.
Values may be sent and summed in bfloat16 or wider, within the bound.
A program may use at most 128 MiB of HBM per device.

v0:
```python
import functools

import jax
import jax.numpy as jnp
from jax import lax
from jax.experimental import pallas as pl
from jax.experimental.pallas import tpu as pltpu
from jax.sharding import PartitionSpec as P

EPS = 1e-06
HIGH = lax.Precision.HIGHEST
LOWEST = -1e30
PIECES = 4
F32 = jnp.float32
BF16 = jnp.bfloat16


def dot(a, b, dims, precision=None):
    return lax.dot_general(a, b, (dims, ((), ())), precision=precision, preferred_element_type=F32)


NN = ((1,), (0,))
NT = ((1,), (1,))
TN = ((0,), (0,))


def ring_place(index, n):
    odd = lax.rem(index, 2)
    half = lax.div(index, 2)
    return (1 - odd) * half + odd * (n - 1 - half)


def ring_index(place, n):
    late = lax.div(place, n // 2)
    return (1 - late) * (2 * place) + late * (2 * (n - 1 - place) + 1)


def pieces(depth):
    return max(1, min(PIECES, depth // 16))


def kernel(
    n,
    t,
    dk,
    dv,
    tokens,
    norm_gain,
    w_query,
    w_key,
    w_value,
    w_conv_b,
    w_conv_c,
    w_conv_in,
    w_out,
    w_gates,
    input_bias,
    forget_bias,
    decay_shift,
    head_gain,
    taps,
    out,
    normed,
    w_all,
    wo_all,
    proj,
    state_out,
    pack_out,
    state_in,
    pack_in,
    carry_c,
    carry_n,
    joined,
    w_ss,
    w_rs,
    wo_ss,
    wo_rs,
    st_ss,
    st_rs,
    pk_ss,
    pk_rs,
    j_ss,
    j_rs,
    own_sem,
    gate_bias,
    decay,
):
    me = lax.axis_index("sp")
    head = lax.axis_index("tp")
    place = ring_place(me, n)
    right = ring_index(lax.rem(place + 1, n), n)
    left = ring_index(lax.rem(place + n - 1, n), n)
    rows = tokens.shape[0]

    parts = (w_query, w_key, w_value, w_conv_b, w_conv_c, w_conv_in)
    copies = []
    offset = 0
    for part in parts:
        depth, cols = part.shape
        spot = w_all.at[pl.ds(pl.multiple_of(me * depth, depth), depth), pl.ds(offset, cols)]
        copies.append(pltpu.make_async_copy(part, spot, own_sem.at[len(copies)]))
        offset += cols
    depth_o = w_out.shape[0]
    spot = wo_all.at[pl.ds(pl.multiple_of(me * depth_o, depth_o), depth_o), :]
    copies.append(pltpu.make_async_copy(w_out, spot, own_sem.at[len(copies)]))
    for copy in copies:
        copy.start()

    barrier = pltpu.get_barrier_semaphore()

    def greet_sp(o, c):
        pl.semaphore_signal(barrier, inc=1, device_id={"sp": lax.rem(me + o, n)})
        return c

    def greet_tp(o, c):
        pl.semaphore_signal(barrier, inc=1, device_id={"tp": lax.rem(head + o, t)})
        return c

    lax.fori_loop(1, n, greet_sp, 0)
    lax.fori_loop(1, t, greet_tp, 0)
    pl.semaphore_wait(barrier, n + t - 2)

    def hop(depth, whole, ss, rs, way, step, piece):
        width = whole.shape[1]
        half, tall = width // 2, depth // pieces(depth)
        holder = ring_index(lax.rem(place + (n + step if way else n - step), n), n)
        columns = pl.ds(way * half, half)
        there = whole.at[pl.ds(pl.multiple_of(holder * depth + piece * tall, tall), tall), columns]
        turn = step * pieces(depth) + piece
        return pltpu.make_async_remote_copy(
            src_ref=there,
            dst_ref=there,
            send_sem=ss.at[way, turn],
            recv_sem=rs.at[way, turn],
            device_id={"sp": left if way else right},
        )

    def ring_start(*ring):
        for piece in range(pieces(ring[0])):
            for way in range(2):
                hop(*ring, way, 0, piece).start()

    def ring_step(step, *ring):
        for piece in range(pieces(ring[0])):
            for way in range(2):
                hop(*ring, way, step - 1, piece).wait_recv()
                hop(*ring, way, step, piece).start()

    def ring_last(*ring):
        for piece in range(pieces(ring[0])):
            for way in range(2):
                hop(*ring, way, n - 2, piece).wait_recv()

    def ring_drain(*ring):
        def drain(step, c):
            for piece in range(pieces(ring[0])):
                for way in range(2):
                    hop(*ring, way, step, piece).wait_send()
            return c

        lax.fori_loop(0, n - 1, drain, 0)

    w_ring = (w_query.shape[0], w_all, w_ss, w_rs)
    wo_ring = (depth_o, wo_all, wo_ss, wo_rs)
    for copy in copies:
        copy.wait()
    ring_start(*w_ring)

    gate_bias[...] = jnp.zeros_like(gate_bias)
    gate_bias[0:2, :] = input_bias[...]
    gate_bias[2:4, :] = forget_bias[...]
    decay[...] = jnp.zeros_like(decay)
    decay[2:4, :] = decay_shift[...]

    chunk = 32

    def norm_rows(i, c):
        span = pl.ds(pl.multiple_of(i * chunk, chunk), chunk)
        values = tokens[span, :].astype(F32)
        inverse = lax.rsqrt(jnp.mean(values * values, axis=-1, keepdims=True) + EPS)
        normed[span, :] = (values * inverse * norm_gain[...]).astype(BF16)
        return c

    lax.fori_loop(0, rows // chunk, norm_rows, 0)

    gates = dot(w_gates[...], normed[...], NT) + gate_bias[...]
    forget = jnp.minimum(gates, 0.0) - jnp.log1p(jnp.exp(-jnp.abs(gates))) + decay[...]
    row_id = lax.broadcasted_iota(jnp.int32, (rows, rows), 0)
    col_id = lax.broadcasted_iota(jnp.int32, (rows, rows), 1)
    upto = (row_id <= col_id).astype(F32)
    after = (row_id >= col_id).astype(F32)
    sums = (dot(forget, upto, NN, HIGH), dot(forget, after, NN, HIGH))
    gates_t = gates.T
    sums_t = (sums[0].T, sums[1].T)

    lax.fori_loop(1, n - 1, lambda s, c: (ring_step(s, *w_ring), c)[1], 0)
    ring_start(*wo_ring)
    ring_last(*w_ring)
    done = [0]

    def advance():
        if done[0] + 1 < n - 1:
            done[0] += 1
            ring_step(done[0], *wo_ring)

    width = 256

    def project(i, c):
        span = pl.ds(pl.multiple_of(i * width, width), width)
        proj[:, span] = dot(normed[...], w_all[:, span], NN).astype(BF16)
        return c

    lax.fori_loop(0, proj.shape[1] // width, project, 0)

    query = proj[:, :dk]
    keys = proj[:, dk : 2 * dk]
    values = proj[:, 2 * dk : 2 * dk + dv]
    base = 2 * dk + dv
    bw = (proj.shape[1] - base) // 3
    mixed = (proj[:, base + bw : base + 2 * bw].astype(F32) * proj[:, base + 2 * bw :].astype(F32)).astype(BF16).astype(F32)

    keys_f = keys.astype(F32)
    totals = []
    for d in range(2):
        cum_c = sums_t[d][:, 2 + d : 3 + d]
        in_c = gates_t[:, d : d + 1]
        last = rows - 1 if d == 0 else 0
        total = cum_c[last : last + 1, :]
        update = total - cum_c + in_c
        stable = jnp.max(update, axis=0, keepdims=True)
        weighted = keys_f * jnp.exp(update - stable)
        state_out[d] = dot(weighted.astype(BF16), values, TN).astype(BF16)
        edge = mixed[rows - 1 :, :] if d == 0 else mixed[:1, :]
        wide = pack_out.shape[-1]
        pack_out[d, 0:1, :] = edge
        pack_out[d, 1:2, :dk] = jnp.sum(weighted, axis=0, keepdims=True)
        pack_out[d, 1:2, dk:] = jnp.zeros((1, wide - dk), F32)
        pack_out[d, 2:3, :] = jnp.broadcast_to(total, (1, wide))
        pack_out[d, 3:4, :] = jnp.broadcast_to(stable, (1, wide))
        pack_out[d, 4:, :] = jnp.zeros((4, wide), F32)

    def give(o):
        other = lax.rem(me + o, n)
        d = lax.div(me + o, n)
        ids = {"sp": other}
        return (
            pltpu.make_async_remote_copy(state_out.at[d], state_in.at[me], st_ss.at[o], st_rs.at[me], device_id=ids),
            pltpu.make_async_remote_copy(pack_out.at[d], pack_in.at[me], pk_ss.at[o], pk_rs.at[me], device_id=ids),
        )

    def take(o):
        source = lax.rem(me + o, n)
        ids = {"sp": source}
        return (
            pltpu.make_async_remote_copy(state_out.at[0], state_in.at[source], st_ss.at[o], st_rs.at[source], device_id=ids),
            pltpu.make_async_remote_copy(pack_out.at[0], pack_in.at[source], pk_ss.at[o], pk_rs.at[source], device_id=ids),
        )

    def give_all(o, c):
        for copy in give(o):
            copy.start()
        return c

    def take_all(o, c):
        for copy in take(o):
            copy.wait_recv()
        return c

    def give_end(o, c):
        for copy in give(o):
            copy.wait_send()
        return c

    lax.fori_loop(1, n, give_all, 0)
    advance()

    scale = dk ** (-0.5)
    scores = dot(query, keys, NT) * scale
    local = []
    for d in range(2):
        cum_c = sums_t[d][:, 2 + d : 3 + d]
        cum_r = sums[d][2 + d : 3 + d, :]
        in_r = gates[d : d + 1, :]
        allowed = row_id >= col_id if d == 0 else row_id <= col_id
        log_weight = jnp.where(allowed, cum_c - cum_r + in_r, -jnp.inf)
        peak = jnp.max(log_weight, axis=-1, keepdims=True)
        part = scores * jnp.exp(log_weight - peak)
        num = dot(part, values.astype(F32), NN, HIGH)
        local.append((cum_c, peak, num, jnp.sum(part, axis=-1, keepdims=True)))
        advance()

    lax.fori_loop(1, n, take_all, 0)

    before = pack_in[lax.rem(me + n - 1, n), 0:1, :] * jnp.minimum(me, 1).astype(F32)
    behind = pack_in[lax.rem(me + 1, n), 0:1, :] * jnp.minimum(n - 1 - me, 1).astype(F32)
    pos = lax.broadcasted_iota(jnp.int32, mixed.shape, 0)
    prior = jnp.where(pos == 0, before, pltpu.roll(mixed, 1, 0))
    later = jnp.where(pos == rows - 1, behind, pltpu.roll(mixed, rows - 1, 0))
    taps_f = taps[...].astype(F32)
    filtered = taps_f[0:1] * prior + taps_f[1:2] * mixed + taps_f[2:3] * later
    joined[head, :, dv:] = (proj[:, base : base + bw].astype(F32) * filtered).astype(BF16)

    def share(part, o, source):
        columns = pl.ds(part * dv, dv)
        slot = joined.at[source, :, columns]
        return pltpu.make_async_remote_copy(
            slot,
            slot,
            j_ss.at[part, o],
            j_rs.at[part, source],
            device_id={"tp": lax.rem(head + o, t)},
        )

    for o in range(1, t):
        share(1, o, head).start()
    advance()

    summed = None
    query_f = query.astype(F32) * scale
    for d in range(2):
        carry_c[...] = jnp.zeros_like(carry_c)
        carry_n[...] = jnp.zeros_like(carry_n)

        def join(i, peak_in):
            source = i if d == 0 else n - 1 - i
            total = pack_in[source, 2:3, :]
            stable = pack_in[source, 3:4, :]
            new = jnp.maximum(peak_in + total, stable)
            old_w = jnp.exp(peak_in + total - new)
            new_w = jnp.exp(stable - new)
            carry_c[...] = old_w * carry_c[...] + new_w * state_in[source].astype(F32)
            carry_n[...] = old_w * carry_n[...] + new_w * pack_in[source, 1:2, :]
            return new

        peak_in = lax.fori_loop(0, me if d == 0 else n - 1 - me, join, jnp.full((1, dv), LOWEST, F32))
        cum_c, peak, num, den = local[d]
        carried = cum_c + peak_in[:, :1]
        top = jnp.maximum(carried, peak)
        carry_w = jnp.exp(carried - top)
        own_w = jnp.exp(peak - top)
        num = own_w * num + carry_w * dot(query_f, carry_c[...], NN, HIGH)
        den = own_w * den + carry_w * jnp.sum(query_f * carry_n[:, :dk], axis=-1, keepdims=True)
        result = num / jnp.maximum(jnp.abs(den), jnp.exp(-top))
        summed = result if d == 0 else summed + result
        if d == 0:
            advance()
    inverse = lax.rsqrt(jnp.mean(summed * summed, axis=-1, keepdims=True) + EPS)
    joined[head, :, :dv] = (summed * inverse * head_gain[...]).astype(BF16)
    for o in range(1, t):
        share(0, o, head).start()

    lax.fori_loop(done[0] + 1, n - 1, lambda s, c: (ring_step(s, *wo_ring), c)[1], 0)
    ring_last(*wo_ring)
    for part in range(2):
        for o in range(1, t):
            share(part, o, lax.rem(head + o, t)).wait_recv()

    span_j = 2 * dv

    def emit(i, c):
        span = pl.ds(pl.multiple_of(i * width, width), width)
        total = dot(joined[0], wo_all[0:span_j, span], NN)
        for j in range(1, t):
            total += dot(joined[j], wo_all[j * span_j : (j + 1) * span_j, span], NN)
        out[:, span] = total.astype(BF16)
        return c

    lax.fori_loop(0, out.shape[1] // width, emit, 0)
    ring_drain(*w_ring)
    ring_drain(*wo_ring)
    lax.fori_loop(1, n, give_end, 0)
    for part in range(2):
        for o in range(1, t):
            share(part, o, head).wait_send()


def body(
    n,
    t,
    tokens,
    norm_gain,
    w_query,
    w_key,
    w_value,
    w_gates,
    input_bias,
    forget_bias,
    decay_shift,
    head_gain,
    w_conv_b,
    w_conv_c,
    w_conv_in,
    conv_taps,
    w_out,
):
    rows, model = tokens.shape
    dk, dv = w_query.shape[1], w_value.shape[1]
    gates = jnp.transpose(w_gates[..., 0], (2, 1, 0)).reshape(4, model)
    gates = jnp.pad(gates, ((0, 4), (0, 0)))
    depth = w_query.shape[0]
    wide, cols = 2 * dk + dv + 3 * w_conv_b.shape[1], w_out.shape[1]
    hbm = pl.BlockSpec(memory_space=pl.ANY)
    vmem = pl.BlockSpec(memory_space=pltpu.VMEM)
    dma = pltpu.SemaphoreType.DMA
    return pl.pallas_call(
        functools.partial(kernel, n, t, dk, dv),
        out_shape=jax.ShapeDtypeStruct((rows, cols), BF16),
        in_specs=[vmem] * 2 + [hbm] * 7 + [vmem] * 6,
        out_specs=vmem,
        scratch_shapes=[
            pltpu.VMEM((rows, model), BF16),
            pltpu.VMEM((n * depth, wide), BF16),
            pltpu.VMEM((n * w_out.shape[0], cols), BF16),
            pltpu.VMEM((rows, wide), BF16),
            pltpu.VMEM((2, dk, dv), BF16),
            pltpu.VMEM((2, 8, dv), F32),
            pltpu.VMEM((n, dk, dv), BF16),
            pltpu.VMEM((n, 8, dv), F32),
            pltpu.VMEM((dk, dv), F32),
            pltpu.VMEM((1, dv), F32),
            pltpu.VMEM((t, rows, 2 * dv), BF16),
            dma((2, (n - 1) * pieces(depth))),
            dma((2, (n - 1) * pieces(depth))),
            dma((2, (n - 1) * pieces(w_out.shape[0]))),
            dma((2, (n - 1) * pieces(w_out.shape[0]))),
            dma((n,)),
            dma((n,)),
            dma((n,)),
            dma((n,)),
            dma((2, t)),
            dma((2, t)),
            dma((7,)),
            pltpu.VMEM((8, 1), F32),
            pltpu.VMEM((8, rows), F32),
        ],
        compiler_params=pltpu.CompilerParams(
            collective_id=0, has_side_effects=True, vmem_limit_bytes=60 * 1024 * 1024
        ),
    )(
        tokens,
        norm_gain.reshape(1, model),
        w_query,
        w_key,
        w_value,
        w_conv_b,
        w_conv_c,
        w_conv_in,
        w_out,
        gates,
        input_bias,
        forget_bias,
        decay_shift[..., 0],
        head_gain.reshape(1, dv),
        conv_taps,
    )


def solution(mesh):
    placed = (
        P("sp", None),
        P(),
        P("sp", "tp"),
        P("sp", "tp"),
        P("sp", "tp"),
        P(None, None, None, "tp"),
        P(None, "tp"),
        P(None, "tp"),
        P(None, "sp", "tp"),
        P("tp"),
        P("sp", "tp"),
        P("sp", "tp"),
        P("sp", "tp"),
        P(None, "tp"),
        P("sp", "tp"),
    )
    step = functools.partial(body, mesh.shape["sp"], mesh.shape["tp"])
    return jax.shard_map(step, mesh=mesh, in_specs=placed, out_specs=P("sp", "tp"), check_vma=False)
```

profile of v0, /device:TPU:0, one launch (start us, length us, event | category | flops | bytes accessed | tf_op | source)
XLA Modules:
  0.0 170.8 jit_solution(8219512467109546086)
XLA Ops:
  0.0 1.3 copy.17.input_bias
  1.3 1.3 copy.18.forget_bias
  2.6 1.3 copy.21
  3.9 0.8 copy.16
  4.7 0.6 pad.4.w_gates
  5.3 163.6 %shard_map.145 = bf16[256,1024]{1,0:T(8,128)(2,1)} custom-call(bf16[256,4096]{1,0:T(8,128)(2,1)} %tokens.1, f32[1,4096]{1,0:T(1,128)} %bitcast.9, bf16[512,128]{1,0:T(8,128)(2,1)} %w_query.1, bf16[512,128]{1,0:T(8,128)(2,1)} %w_key.1, bf16[512,256]{1,0:T(8,128)(2,1)} %w_value.1, bf16[512,256]{1,0:T(8,128)(2,1)} %w_conv_b.1, bf16[512,256]{1,0:T(8,128)(2,1)} %w_conv_c.1, ...), custom_call_target="tpu_custom_call" | custom-call | tf_op jit(solution)/shard_map/pallas_call | solution.py:405
  168.9 1.9 %copy.23 = bf16[256,1024]{1,0:T(8,128)(2,1)} copy(bf16[256,1024]{1,0:T(8,128)(2,1)} %shard_map.145) | data formatting | bytes 1048576
  (1 shorter events, 0.0 us)
where the time goes:
time: 171 us
  Pallas kernels  164 us (96%)
  local copies, waits for them, and re-layouts  7.19 us (4%)
    pallas_call x1, Pallas kernels, body(): pl.pallas_call(functools.partial(kernel, n, t, dk, dv), out_shape=jax.Sha...  164 us
    unnamed x4, local copies, waits for them, and re-layouts  5.73 us

commit v1 on v0

--- a/solution.py
+++ b/solution.py
@@ -39,7 +39,7 @@
     return max(1, min(PIECES, depth // 16))
 
 
-def kernel(
+def gather_kernel(
     n,
     t,
     dk,
@@ -374,7 +374,7 @@
             share(part, o, head).wait_send()
 
 
-def body(
+def gather_body(
     n,
     t,
     tokens,
@@ -403,7 +403,7 @@
     vmem = pl.BlockSpec(memory_space=pltpu.VMEM)
     dma = pltpu.SemaphoreType.DMA
     return pl.pallas_call(
-        functools.partial(kernel, n, t, dk, dv),
+        functools.partial(gather_kernel, n, t, dk, dv),
         out_shape=jax.ShapeDtypeStruct((rows, cols), BF16),
         in_specs=[vmem] * 2 + [hbm] * 7 + [vmem] * 6,
         out_specs=vmem,
@@ -455,6 +455,709 @@
     )
 
 
+PAIR = 2
+WO_PIECES = 2
+
+
+def fits(n, t, tokens, norm_gain, w_query, w_key, w_value, *rest):
+    w_conv, w_out = rest[5], rest[9]
+    depth, dk = w_query.shape
+    dv = w_value.shape[1]
+    rows = tokens.shape[0]
+    even = n % PAIR == 0 and n > PAIR and t == 4
+    wide = 2 * dk == dv and w_conv.shape[1] == dv and dv % 128 == 0 and dk % 128 == 0
+    deep = (PAIR * depth) % (t * 128) == 0 and rows % 32 == 0 and w_out.shape[0] % (16 * WO_PIECES) == 0
+    return even and wide and deep and rows <= depth
+
+
+def kernel(
+    n,
+    t,
+    dk,
+    dv,
+    tokens,
+    norm_gain,
+    w_query,
+    w_key,
+    w_value,
+    w_conv_b,
+    w_conv_c,
+    w_conv_in,
+    w_out,
+    w_gates,
+    input_bias,
+    forget_bias,
+    decay_shift,
+    head_gain,
+    taps,
+    out,
+    tok,
+    nbuf,
+    tall,
+    wbuf,
+    wo_all,
+    acc,
+    sbuf,
+    rbuf,
+    proj,
+    wg,
+    decay,
+    state_out,
+    pack_out,
+    state_in,
+    pack_in,
+    edge_out,
+    edge_in,
+    carry_c,
+    carry_n,
+    local_num,
+    joined,
+    own_sem,
+    tk_ss,
+    tk_rs,
+    tf_ss,
+    tf_rs,
+    w_ss,
+    w_rs,
+    rs_ss,
+    rs_rs,
+    st_ss,
+    st_rs,
+    pk_ss,
+    pk_rs,
+    ed_ss,
+    ed_rs,
+    j_ss,
+    j_rs,
+    oz_ss,
+    oz_rs,
+    oy_ss,
+    oy_rs,
+):
+    me = lax.axis_index("sp")
+    head = lax.axis_index("tp")
+    lines = n // PAIR
+    z = lax.div(me, PAIR)
+    y = lax.rem(me, PAIR)
+    mate = me + 1 - 2 * y
+    core = lax.rem(head, 2)
+    core_mate = head + 1 - 2 * core
+    x_mate = lax.rem(head + 2, t)
+    far_mate = lax.rem(core_mate + 2, t)
+    rows, model = tokens.shape
+    depth = w_query.shape[0]
+    part_k = nbuf.shape[-1]
+    chunks = wbuf.shape[0]
+
+    def at_line(line):
+        return PAIR * line + y
+
+    load_tok = pltpu.make_async_copy(tokens, tok, own_sem.at[0])
+    load_tok.start()
+    mine = pl.ds(pl.multiple_of(y * depth, depth), depth)
+    loads = []
+    plan = ((w_query, 0, 0), (w_key, 0, dk), (w_value, 1, 0), (w_conv_c, 2, 0), (w_conv_in, 3, 0), (w_conv_b, 4, 0))
+    for part, chunk, offset in plan:
+        spot = wbuf.at[chunk, mine, pl.ds(offset, part.shape[1])]
+        loads.append(pltpu.make_async_copy(part, spot, own_sem.at[1 + len(loads)]))
+    depth_o = w_out.shape[0]
+    spot = wo_all.at[pl.ds(pl.multiple_of(me * depth_o, depth_o), depth_o), :]
+    loads.append(pltpu.make_async_copy(w_out, spot, own_sem.at[1 + len(loads)]))
+    for load in loads:
+        load.start()
+
+    edge_in[...] = jnp.zeros_like(edge_in)
+
+    barrier = pltpu.get_barrier_semaphore()
+
+    def greet_sp(o, c):
+        pl.semaphore_signal(barrier, inc=1, device_id={"sp": lax.rem(me + o, n)})
+        return c
+
+    def greet_tp(o, c):
+        pl.semaphore_signal(barrier, inc=1, device_id={"tp": lax.rem(head + o, t)})
+        return c
+
+    lax.fori_loop(1, n, greet_sp, 0)
+    lax.fori_loop(1, t, greet_tp, 0)
+
+    load_tok.wait()
+    rows_at_once = 32
+
+    def norm_rows(i, c):
+        span = pl.ds(pl.multiple_of(i * rows_at_once, rows_at_once), rows_at_once)
+        values = tok[span, :].astype(F32)
+        inverse = lax.rsqrt(jnp.mean(values * values, axis=-1, keepdims=True) + EPS)
+        normed = (values * inverse * norm_gain[...]).astype(BF16)
+        for b in range(lines * t):
+            nbuf[b // t, b % t, span, :] = normed[:, b * part_k : (b + 1) * part_k]
+        return c
+
+    lax.fori_loop(0, rows // rows_at_once, norm_rows, 0)
+    pl.semaphore_wait(barrier, n + t - 2)
+
+    ups = lines - 1 - z
+
+    def pick(k, near):
+        up = jnp.clip(ups - k, 0, 1)
+        down_k = k - ups
+        if near:
+            return up, up * (z + 1 + k) + (1 - up) * (z - 1 - down_k)
+        return up, up * (lines - 1 - k) + (1 - up) * down_k
+
+    def token_send(line):
+        return pltpu.make_async_remote_copy(
+            nbuf.at[line, head], tall.at[z, head], tk_ss.at[line], tk_rs.at[z], device_id={"sp": at_line(line)}
+        )
+
+    def token_take(line):
+        return pltpu.make_async_remote_copy(
+            nbuf.at[line, head], tall.at[line, head], tk_ss.at[line], tk_rs.at[line], device_id={"sp": at_line(line)}
+        )
+
+    def token_pass(line, way):
+        quarter = (head, head, x_mate)[way]
+        there = tall.at[line, quarter]
+        return pltpu.make_async_remote_copy(
+            there, there, tf_ss.at[way, line], tf_rs.at[way, line], device_id={"tp": (core_mate, x_mate, core_mate)[way]}
+        )
+
+    def token_get(line, way):
+        quarter = (core_mate, x_mate, far_mate)[way]
+        there = tall.at[line, quarter]
+        return pltpu.make_async_remote_copy(
+            there, there, tf_ss.at[way, line], tf_rs.at[way, line], device_id={"tp": (core_mate, x_mate, core_mate)[way]}
+        )
+
+    def send_tokens(k, c):
+        _, line = pick(k, False)
+        token_send(line).start()
+        return c
+
+    lax.fori_loop(0, lines - 1, send_tokens, 0)
+
+    def w_send(chunk):
+        there = wbuf.at[chunk, mine, :]
+        return pltpu.make_async_remote_copy(there, there, w_ss.at[chunk], w_rs.at[chunk], device_id={"sp": mate})
+
+    def w_take(chunk):
+        there = wbuf.at[chunk, pl.ds(pl.multiple_of((1 - y) * depth, depth), depth), :]
+        return pltpu.make_async_remote_copy(there, there, w_ss.at[chunk], w_rs.at[chunk], device_id={"sp": mate})
+
+    for load in loads:
+        load.wait()
+    for chunk in range(chunks):
+        w_send(chunk).start()
+
+    tall_o = depth_o // WO_PIECES
+
+    def wo_rows(index, piece):
+        return wo_all.at[pl.ds(pl.multiple_of(index * depth_o + piece * tall_o, tall_o), tall_o), :]
+
+    def wo_line(line, piece, way, sem):
+        there = wo_rows(at_line(line), piece)
+        return pltpu.make_async_remote_copy(
+            there, there, oz_ss.at[sem, piece], oz_rs.at[line, piece], device_id={"sp": at_line(z + way)}
+        )
+
+    def wo_mate(line, piece):
+        there = wo_rows(at_line(line), piece)
+        return pltpu.make_async_remote_copy(
+            there, there, oy_ss.at[line, piece], oy_rs.at[line, piece], device_id={"sp": mate}
+        )
+
+    def wo_mate_take(line, piece):
+        there = wo_rows(PAIR * line + 1 - y, piece)
+        return pltpu.make_async_remote_copy(
+            there, there, oy_ss.at[line, piece], oy_rs.at[line, piece], device_id={"sp": mate}
+        )
+
+    def wo_own(way, wanted):
+        @pl.when(wanted)
+        def _():
+            for piece in range(WO_PIECES):
+                wo_line(z, piece, way, lines + (way + 1) // 2).start()
+
+    half_way = lines // 2
+    has_up, has_down = z < lines - 1, z > 0
+    at_end = jnp.logical_or(z == 0, z == lines - 1)
+    upper = z >= half_way
+
+    def wo_outward():
+        wo_own(1, jnp.logical_and(upper, has_up))
+        wo_own(-1, jnp.logical_and(jnp.logical_not(upper), has_down))
+
+    def wo_inward(ends):
+        here = at_end if ends else jnp.logical_not(at_end)
+        wo_own(-1, jnp.logical_and(jnp.logical_and(upper, has_down), here))
+        wo_own(1, jnp.logical_and(jnp.logical_and(jnp.logical_not(upper), has_up), here))
+
+    def wo_relay(line):
+        @pl.when(z != line)
+        def _():
+            for piece in range(WO_PIECES):
+                wo_line(line, piece, 0, line).wait_recv()
+
+                @pl.when(jnp.logical_and(z > line, has_up))
+                def _():
+                    wo_line(line, piece, 1, line).start()
+
+                @pl.when(jnp.logical_and(z < line, has_down))
+                def _():
+                    wo_line(line, piece, -1, line).start()
+
+                wo_mate(line, piece).start()
+
+    for piece in range(WO_PIECES):
+        wo_mate(z, piece).start()
+    wo_outward()
+
+    wg[...] = jnp.zeros_like(wg)
+    wg[0:2, :] = w_gates[0]
+    wg[2:4, :] = w_gates[1]
+    decay[...] = jnp.zeros_like(decay)
+    decay[1:2, :] = decay_shift[0]
+    decay[3:4, :] = decay_shift[1]
+    gates = None
+    for b in range(lines * t):
+        piece = dot(wg[:, b * part_k : (b + 1) * part_k], nbuf[b // t, b % t], NT)
+        gates = piece if b == 0 else gates + piece
+    gate_id = lax.broadcasted_iota(jnp.int32, gates.shape, 0)
+    offsets = (input_bias[0, 0], forget_bias[0, 0], input_bias[0, 1], forget_bias[0, 1])
+    for i, offset in enumerate(offsets):
+        gates = jnp.where(gate_id == i, gates + offset, gates)
+    forget = jnp.minimum(gates, 0.0) - jnp.log1p(jnp.exp(-jnp.abs(gates))) + decay[...]
+    row_id = lax.broadcasted_iota(jnp.int32, (rows, rows), 0)
+    col_id = lax.broadcasted_iota(jnp.int32, (rows, rows), 1)
+    upto = (row_id <= col_id).astype(F32)
+    after = (row_id >= col_id).astype(F32)
+    sums = (dot(forget, upto, NN, HIGH), dot(forget, after, NN, HIGH))
+    gates_t = gates.T
+    sums_t = (sums[0].T, sums[1].T)
+
+    def relay_direct(k, c):
+        _, line = pick(k, True)
+        token_take(line).wait_recv()
+        token_pass(line, 1).start()
+        token_pass(line, 0).start()
+        return c
+
+    def relay_across(k, c):
+        _, line = pick(k, True)
+        token_get(line, 1).wait_recv()
+        token_pass(line, 2).start()
+        return c
+
+    def tokens_ready(k, c):
+        _, line = pick(k, True)
+        token_get(line, 0).wait_recv()
+        token_get(line, 2).wait_recv()
+        return c
+
+    lax.fori_loop(0, lines - 1, relay_direct, 0)
+    lax.fori_loop(0, lines - 1, relay_across, 0)
+    lax.fori_loop(0, lines - 1, tokens_ready, 0)
+
+    def product(source, line, chunk):
+        total = dot(source[line, 0], wbuf[chunk, 0:part_k, :], NN)
+        for q in range(1, t):
+            total += dot(source[line, q], wbuf[chunk, q * part_k : (q + 1) * part_k, :], NN)
+        return total
+
+    def hop(chunk, k, near):
+        up, line = pick(k, near)
+        last = (1 - up) * (1 - jnp.minimum(jnp.abs(z - line) - 1, 1))
+        slot = line + last * (lines - line)
+        copy = pltpu.make_async_remote_copy(
+            sbuf.at[chunk, k], rbuf.at[chunk, slot], rs_ss.at[chunk, k], rs_rs.at[chunk, slot],
+            device_id={"sp": at_line(z + 2 * up - 1)},
+        )
+        return up, line, copy
+
+    def arrived(chunk, slot):
+        return pltpu.make_async_remote_copy(
+            sbuf.at[chunk, 0], rbuf.at[chunk, slot], rs_ss.at[chunk, 0], rs_rs.at[chunk, slot], device_id={"sp": me}
+        )
+
+    def reduce_chunk(chunk):
+        near = chunk == 0
+
+        def one(k, c):
+            up, line, copy = hop(chunk, k, near)
+            acc[...] = product(tall, line, chunk)
+            before = up * jnp.minimum(z, 1) + (1 - up) * jnp.minimum(ups, 1)
+
+            @pl.when(before == 1)
+            def _():
+                arrived(chunk, line).wait_recv()
+                sbuf[chunk, k] = (acc[...] + rbuf[chunk, line].astype(F32)).astype(BF16)
+
+            @pl.when(before == 0)
+            def _():
+                sbuf[chunk, k] = acc[...].astype(BF16)
+
+            copy.start()
+            return c
+
+        w_take(chunk).wait_recv()
+        lax.fori_loop(0, lines - 1, one, 0)
+
+    def own_chunk(chunk):
+        acc[...] = product(nbuf, z, chunk)
+
+        @pl.when(has_down)
+        def _():
+            arrived(chunk, z).wait_recv()
+            acc[...] += rbuf[chunk, z].astype(F32)
+
+        @pl.when(has_up)
+        def _():
+            arrived(chunk, lines).wait_recv()
+            acc[...] += rbuf[chunk, lines].astype(F32)
+
+        proj[chunk] = acc[...].astype(BF16)
+
+    reduce_chunk(0)
+    reduce_chunk(1)
+    wo_inward(False)
+    own_chunk(0)
+    reduce_chunk(2)
+    own_chunk(1)
+
+    keys_f = proj[0, :, dk:].astype(F32)
+    wide = pack_out.shape[-1]
+    for d in range(2):
+        cum_c = sums_t[d][:, 2 * d + 1 : 2 * d + 2]
+        in_c = gates_t[:, 2 * d : 2 * d + 1]
+        last = rows - 1 if d == 0 else 0
+        total = cum_c[last : last + 1, :]
+        update = total - cum_c + in_c
+        stable = jnp.max(update, axis=0, keepdims=True)
+        weighted = keys_f * jnp.exp(update - stable)
+        state_out[d] = dot(weighted.astype(BF16), proj[1], TN).astype(BF16)
+        pack_out[d, 0:1, :dk] = jnp.sum(weighted, axis=0, keepdims=True)
+        pack_out[d, 0:1, dk:] = jnp.zeros((1, wide - dk), F32)
+        pack_out[d, 1:2, :] = jnp.broadcast_to(total, (1, wide))
+        pack_out[d, 2:3, :] = jnp.broadcast_to(stable, (1, wide))
+        pack_out[d, 3:, :] = jnp.zeros((5, wide), F32)
+
+    def give(o):
+        other = lax.rem(me + o, n)
+        d = lax.div(me + o, n)
+        ids = {"sp": other}
+        return (
+            pltpu.make_async_remote_copy(state_out.at[d], state_in.at[me], st_ss.at[o], st_rs.at[me], device_id=ids),
+            pltpu.make_async_remote_copy(pack_out.at[d], pack_in.at[me], pk_ss.at[o], pk_rs.at[me], device_id=ids),
+        )
+
+    def take(o):
+        source = lax.rem(me + o, n)
+        ids = {"sp": source}
+        return (
+            pltpu.make_async_remote_copy(state_out.at[0], state_in.at[source], st_ss.at[o], st_rs.at[source], device_id=ids),
+            pltpu.make_async_remote_copy(pack_out.at[0], pack_in.at[source], pk_ss.at[o], pk_rs.at[source], device_id=ids),
+        )
+
+    def give_all(o, c):
+        for copy in give(o):
+            copy.start()
+        return c
+
+    def take_all(o, c):
+        for copy in take(o):
+            copy.wait_recv()
+        return c
+
+    def give_end(o, c):
+        for copy in give(o):
+            copy.wait_send()
+        return c
+
+    lax.fori_loop(1, n, give_all, 0)
+
+    reduce_chunk(3)
+    own_chunk(2)
+
+    scale = dk ** (-0.5)
+    scores = dot(proj[0, :, :dk], proj[0, :, dk:], NT) * scale
+    local = []
+    for d in range(2):
+        cum_c = sums_t[d][:, 2 * d + 1 : 2 * d + 2]
+        cum_r = sums[d][2 * d + 1 : 2 * d + 2, :]
+        in_r = gates[2 * d : 2 * d + 1, :]
+        allowed = row_id >= col_id if d == 0 else row_id <= col_id
+        log_weight = jnp.where(allowed, cum_c - cum_r + in_r, -jnp.inf)
+        peak = jnp.max(log_weight, axis=-1, keepdims=True)
+        part = scores * jnp.exp(log_weight - peak)
+        local_num[d] = dot(part.astype(BF16), proj[1], NN)
+        local.append((cum_c, peak, jnp.sum(part, axis=-1, keepdims=True)))
+
+    reduce_chunk(4)
+    wo_inward(True)
+    own_chunk(3)
+
+    mixed = (proj[2].astype(F32) * proj[3].astype(F32)).astype(BF16).astype(F32)
+    edge_out[0, 0:1, :] = mixed[rows - 1 :, :]
+    edge_out[1, 0:1, :] = mixed[:1, :]
+    edge_out[0, 1:, :] = jnp.zeros((7, dv), F32)
+    edge_out[1, 1:, :] = jnp.zeros((7, dv), F32)
+
+    def edge(way):
+        other = me + 1 if way == 0 else me - 1
+        return pltpu.make_async_remote_copy(
+            edge_out.at[way], edge_in.at[way], ed_ss.at[way], ed_rs.at[way], device_id={"sp": other}
+        )
+
+    later_exists, prior_exists = me < n - 1, me > 0
+
+    @pl.when(later_exists)
+    def _():
+        edge(0).start()
+
+    @pl.when(prior_exists)
+    def _():
+        edge(1).start()
+
+    for line in range(1, lines - 1):
+        wo_relay(line)
+
+    def share(part, o, source):
+        columns = pl.ds(part * dv, dv)
+        slot = joined.at[source, :, columns]
+        return pltpu.make_async_remote_copy(
+            slot,
+            slot,
+            j_ss.at[part, o],
+            j_rs.at[part, source],
+            device_id={"tp": lax.rem(head + o, t)},
+        )
+
+    lax.fori_loop(1, n, take_all, 0)
+    summed = None
+    query_f = proj[0, :, :dk].astype(F32) * scale
+    for d in range(2):
+        carry_c[...] = jnp.zeros_like(carry_c)
+        carry_n[...] = jnp.zeros_like(carry_n)
+
+        def join(i, peak_in):
+            source = i if d == 0 else n - 1 - i
+            total = pack_in[source, 1:2, :]
+            stable = pack_in[source, 2:3, :]
+            new = jnp.maximum(peak_in + total, stable)
+            old_w = jnp.exp(peak_in + total - new)
+            new_w = jnp.exp(stable - new)
+            carry_c[...] = old_w * carry_c[...] + new_w * state_in[source].astype(F32)
+            carry_n[...] = old_w * carry_n[...] + new_w * pack_in[source, 0:1, :]
+            return new
+
+        peak_in = lax.fori_loop(0, me if d == 0 else n - 1 - me, join, jnp.full((1, dv), LOWEST, F32))
+        cum_c, peak, den = local[d]
+        carried = cum_c + peak_in[:, :1]
+        top = jnp.maximum(carried, peak)
+        carry_w = jnp.exp(carried - top)
+        own_w = jnp.exp(peak - top)
+        num = own_w * local_num[d] + carry_w * dot(query_f.astype(BF16), carry_c[...].astype(BF16), NN)
+        den = own_w * den + carry_w * jnp.sum(query_f * carry_n[:, :dk], axis=-1, keepdims=True)
+        result = num / jnp.maximum(jnp.abs(den), jnp.exp(-top))
+        summed = result if d == 0 else summed + result
+    inverse = lax.rsqrt(jnp.mean(summed * summed, axis=-1, keepdims=True) + EPS)
+    joined[head, :, :dv] = (summed * inverse * head_gain[...]).astype(BF16)
+    for o in range(1, t):
+        share(0, o, head).start()
+
+    own_chunk(4)
+
+    @pl.when(prior_exists)
+    def _():
+        edge(0).wait_recv()
+
+    @pl.when(later_exists)
+    def _():
+        edge(1).wait_recv()
+
+    mixed = (proj[2].astype(F32) * proj[3].astype(F32)).astype(BF16).astype(F32)
+    pos = lax.broadcasted_iota(jnp.int32, mixed.shape, 0)
+    prior = jnp.where(pos == 0, edge_in[0, 0:1, :], pltpu.roll(mixed, 1, 0))
+    later = jnp.where(pos == rows - 1, edge_in[1, 0:1, :], pltpu.roll(mixed, rows - 1, 0))
+    taps_f = taps[...].astype(F32)
+    filtered = taps_f[0:1] * prior + taps_f[1:2] * mixed + taps_f[2:3] * later
+    joined[head, :, dv:] = (proj[4].astype(F32) * filtered).astype(BF16)
+    for o in range(1, t):
+        share(1, o, head).start()
+
+    wo_relay(0)
+    wo_relay(lines - 1)
+
+    for line in range(lines):
+        for piece in range(WO_PIECES):
+            wo_mate_take(line, piece).wait_recv()
+    for part in range(2):
+        for o in range(1, t):
+            share(part, o, lax.rem(head + o, t)).wait_recv()
+
+    span_j = 2 * dv
+    width = 256
+
+    def emit(i, c):
+        span = pl.ds(pl.multiple_of(i * width, width), width)
+        total = dot(joined[0], wo_all[0:span_j, span], NN)
+        for j in range(1, t):
+            total += dot(joined[j], wo_all[j * span_j : (j + 1) * span_j, span], NN)
+        out[:, span] = total.astype(BF16)
+        return c
+
+    lax.fori_loop(0, out.shape[1] // width, emit, 0)
+
+    def token_end(k, c):
+        _, line = pick(k, False)
+        token_send(line).wait_send()
+        for way in range(3):
+            token_pass(line, way).wait_send()
+        for chunk in range(chunks):
+            hop(chunk, k, chunk == 0)[2].wait_send()
+        return c
+
+    lax.fori_loop(0, lines - 1, token_end, 0)
+    for chunk in range(chunks):
+        w_send(chunk).wait_send()
+    lax.fori_loop(1, n, give_end, 0)
+
+    @pl.when(later_exists)
+    def _():
+        edge(0).wait_send()
+
+    @pl.when(prior_exists)
+    def _():
+        edge(1).wait_send()
+
+    for part in range(2):
+        for o in range(1, t):
+            share(part, o, head).wait_send()
+    for piece in range(WO_PIECES):
+
+        @pl.when(has_up)
+        def _():
+            wo_line(z, piece, 1, lines + 1).wait_send()
+
+        @pl.when(has_down)
+        def _():
+            wo_line(z, piece, -1, lines).wait_send()
+
+        for line in range(lines):
+
+            @pl.when(jnp.logical_and(z > line, has_up))
+            def _():
+                wo_line(line, piece, 1, line).wait_send()
+
+            @pl.when(jnp.logical_and(z < line, has_down))
+            def _():
+                wo_line(line, piece, -1, line).wait_send()
+
+            wo_mate(line, piece).wait_send()
+
+
+def body(
+    n,
+    t,
+    tokens,
+    norm_gain,
+    w_query,
+    w_key,
+    w_value,
+    w_gates,
+    input_bias,
+    forget_bias,
+    decay_shift,
+    head_gain,
+    w_conv_b,
+    w_conv_c,
+    w_conv_in,
+    conv_taps,
+    w_out,
+):
+    rows, model = tokens.shape
+    depth, dk = w_query.shape
+    dv = w_value.shape[1]
+    lines = n // PAIR
+    chunks = 5
+    part_k = PAIR * depth // t
+    cols = w_out.shape[1]
+    gates = jnp.transpose(w_gates[..., 0], (1, 2, 0))
+    hbm = pl.BlockSpec(memory_space=pl.ANY)
+    vmem = pl.BlockSpec(memory_space=pltpu.VMEM)
+    smem = pl.BlockSpec(memory_space=pltpu.SMEM)
+    dma = pltpu.SemaphoreType.DMA
+    return pl.pallas_call(
+        functools.partial(kernel, n, t, dk, dv),
+        out_shape=jax.ShapeDtypeStruct((rows, cols), BF16),
+        in_specs=[hbm, vmem] + [hbm] * 7 + [vmem] + [smem] * 2 + [vmem] * 3,
+        out_specs=vmem,
+        scratch_shapes=[
+            pltpu.VMEM((rows, model), BF16),
+            pltpu.VMEM((lines, t, rows, part_k), BF16),
+            pltpu.VMEM((lines, t, rows, part_k), BF16),
+            pltpu.VMEM((chunks, PAIR * depth, dv), BF16),
+            pltpu.VMEM((n * w_out.shape[0], cols), BF16),
+            pltpu.VMEM((rows, dv), F32),
+            pltpu.VMEM((chunks, lines - 1, rows, dv), BF16),
+            pltpu.VMEM((chunks, lines + 1, rows, dv), BF16),
+            pltpu.VMEM((chunks, rows, dv), BF16),
+            pltpu.VMEM((8, model), BF16),
+            pltpu.VMEM((8, rows), F32),
+            pltpu.VMEM((2, dk, dv), BF16),
+            pltpu.VMEM((2, 8, dv), F32),
+            pltpu.VMEM((n, dk, dv), BF16),
+            pltpu.VMEM((n, 8, dv), F32),
+            pltpu.VMEM((2, 8, dv), F32),
+            pltpu.VMEM((2, 8, dv), F32),
+            pltpu.VMEM((dk, dv), F32),
+            pltpu.VMEM((1, dv), F32),
+            pltpu.VMEM((2, rows, dv), F32),
+            pltpu.VMEM((t, rows, 2 * dv), BF16),
+            dma((8,)),
+            dma((lines,)),
+            dma((lines,)),
+            dma((3, lines)),
+            dma((3, lines)),
+            dma((chunks,)),
+            dma((chunks,)),
+            dma((chunks, lines - 1)),
+            dma((chunks, lines + 1)),
+            dma((n,)),
+            dma((n,)),
+            dma((n,)),
+            dma((n,)),
+            dma((2,)),
+            dma((2,)),
+            dma((2, t)),
+            dma((2, t)),
+            dma((lines + 2, WO_PIECES)),
+            dma((lines, WO_PIECES)),
+            dma((lines, WO_PIECES)),
+            dma((lines, WO_PIECES)),
+        ],
+        compiler_params=pltpu.CompilerParams(
+            collective_id=0, has_side_effects=True, vmem_limit_bytes=60 * 1024 * 1024
+        ),
+    )(
+        tokens,
+        norm_gain.reshape(1, model),
+        w_query,
+        w_key,
+        w_value,
+        w_conv_b,
+        w_conv_c,
+        w_conv_in,
+        w_out,
+        gates,
+        input_bias.T,
+        forget_bias.T,
+        jnp.swapaxes(decay_shift, 1, 2),
+        head_gain.reshape(1, dv),
+        conv_taps,
+    )
+
+
 def solution(mesh):
     placed = (
         P("sp", None),
@@ -473,5 +1176,10 @@
         P(None, "tp"),
         P("sp", "tp"),
     )
-    step = functools.partial(body, mesh.shape["sp"], mesh.shape["tp"])
+    n, t = mesh.shape["sp"], mesh.shape["tp"]
+
+    def step(*args):
+        form = body if fits(n, t, *args) else gather_body
+        return form(n, t, *args)
+
     return jax.shard_map(step, mesh=mesh, in_specs=placed, out_specs=P("sp", "tp"), check_vma=False)

time: 171 us -> 146 us (0.85)
  Pallas kernels: 164 us -> 144 us
  local copies, waits for them, and re-layouts: 7.19 us -> 1.87 us
    pallas_call x1, Pallas kernels: 164 us -> 144 us  [body(): pl.pallas_call(functools.partial(kernel, n, t, dk, dv), out_shape=jax.Sha...]
    unnamed x4 -> x1, local copies, waits for them, and re-layouts: 5.73 us -> 1.87 us
where the time goes in v1:
time: 146 us
  Pallas kernels  144 us (99%)
  local copies, waits for them, and re-layouts  1.87 us (1%)
    pallas_call x1, Pallas kernels, body(): pl.pallas_call(functools.partial(kernel, n, t, dk, dv), out_shape=jax.Sha...  144 us

profile of v1, /device:TPU:0, one launch (start us, length us, event | category | flops | bytes accessed | tf_op | source)
XLA Modules:
  0.0 145.8 jit_solution(1010208110509642492)
XLA Ops:
  0.0 143.9 %shard_map.145 = bf16[256,1024]{1,0:T(8,128)(2,1)} custom-call(bf16[256,4096]{1,0:T(8,128)(2,1)} %tokens.1, f32[1,4096]{1,0:T(1,128)} %bitcast.9, bf16[512,128]{1,0:T(8,128)(2,1)} %w_query.1, bf16[512,128]{1,0:T(8,128)(2,1)} %w_key.1, bf16[512,256]{1,0:T(8,128)(2,1)} %w_value.1, bf16[512,256]{1,0:T(8,128)(2,1)} %w_conv_b.1, bf16[512,256]{1,0:T(8,128)(2,1)} %w_conv_c.1, ...), custom_call_target="tpu_custom_call" | custom-call | tf_op jit(solution)/shard_map/pallas_call | solution.py:1090
  143.9 1.9 %copy.17 = bf16[256,1024]{1,0:T(8,128)(2,1)} copy(bf16[256,1024]{1,0:T(8,128)(2,1)} %shard_map.145) | data formatting | bytes 1048576

commit v2 on v1

--- a/solution.py
+++ b/solution.py
@@ -504,6 +504,10 @@
     decay,
     state_out,
     pack_out,
+    mate_state,
+    mate_pack,
+    pair_state,
+    pair_pack,
     state_in,
     pack_in,
     edge_out,
@@ -598,6 +602,11 @@
 
     ups = lines - 1 - z
 
+    half_way = lines // 2
+    end_here = 1 - jnp.minimum(z, 1) * jnp.minimum(ups, 1)
+    inner_up = jnp.minimum(lax.div(ups, half_way), 1)
+    inner_count = inner_up * ups + (1 - inner_up) * z
+
     def pick(k, near):
         up = jnp.clip(ups - k, 0, 1)
         down_k = k - ups
@@ -678,7 +687,6 @@
             for piece in range(WO_PIECES):
                 wo_line(z, piece, way, lines + (way + 1) // 2).start()
 
-    half_way = lines // 2
     has_up, has_down = z < lines - 1, z > 0
     at_end = jnp.logical_or(z == 0, z == lines - 1)
     upper = z >= half_way
@@ -692,25 +700,39 @@
         wo_own(-1, jnp.logical_and(jnp.logical_and(upper, has_down), here))
         wo_own(1, jnp.logical_and(jnp.logical_and(jnp.logical_not(upper), has_up), here))
 
-    def wo_relay(line):
-        @pl.when(z != line)
+    def wo_relay(line, wanted, along, across, pieces_now=range(WO_PIECES)):
+        @pl.when(jnp.logical_and(wanted, jnp.logical_and(line >= 0, line < lines)))
         def _():
-            for piece in range(WO_PIECES):
-                wo_line(line, piece, 0, line).wait_recv()
-
-                @pl.when(jnp.logical_and(z > line, has_up))
-                def _():
-                    wo_line(line, piece, 1, line).start()
-
-                @pl.when(jnp.logical_and(z < line, has_down))
-                def _():
-                    wo_line(line, piece, -1, line).start()
-
-                wo_mate(line, piece).start()
+            for piece in pieces_now:
+                if along:
+                    wo_line(line, piece, 0, line).wait_recv()
+
+                    @pl.when(jnp.logical_and(line < z, has_up))
+                    def _():
+                        wo_line(line, piece, 1, line).start()
+
+                    @pl.when(jnp.logical_and(line > z, has_down))
+                    def _():
+                        wo_line(line, piece, -1, line).start()
+
+                if across:
+                    wo_mate(line, piece).start()
+
+    inner_way = 2 * inner_up - 1
+
+    def wo_first(pieces_now):
+        wo_relay(z - inner_way * (1 - 2 * end_here), True, True, True, pieces_now)
+
+    def wo_second(along, across):
+        wo_relay(z + inner_way, jnp.logical_not(at_end), along, across)
+
+    def wo_rest(away, pieces_now):
+        wo_relay(z - away, True, True, True, pieces_now)
+        wo_relay(z + away, True, True, True, pieces_now)
 
     for piece in range(WO_PIECES):
         wo_mate(z, piece).start()
-    wo_outward()
+    wo_inward(True)
 
     wg[...] = jnp.zeros_like(wg)
     wg[0:2, :] = w_gates[0]
@@ -755,52 +777,70 @@
         return c
 
     lax.fori_loop(0, lines - 1, relay_direct, 0)
+    wo_outward()
+    wo_inward(False)
     lax.fori_loop(0, lines - 1, relay_across, 0)
     lax.fori_loop(0, lines - 1, tokens_ready, 0)
-
     def product(source, line, chunk):
         total = dot(source[line, 0], wbuf[chunk, 0:part_k, :], NN)
         for q in range(1, t):
             total += dot(source[line, q], wbuf[chunk, q * part_k : (q + 1) * part_k, :], NN)
         return total
 
-    def hop(chunk, k, near):
-        up, line = pick(k, near)
+    def hop(chunk, k, up, line):
         last = (1 - up) * (1 - jnp.minimum(jnp.abs(z - line) - 1, 1))
         slot = line + last * (lines - line)
-        copy = pltpu.make_async_remote_copy(
-            sbuf.at[chunk, k], rbuf.at[chunk, slot], rs_ss.at[chunk, k], rs_rs.at[chunk, slot],
+        return pltpu.make_async_remote_copy(
+            sbuf.at[chunk, k],
+            rbuf.at[chunk, slot],
+            rs_ss.at[chunk, k],
+            rs_rs.at[chunk, slot],
             device_id={"sp": at_line(z + 2 * up - 1)},
         )
-        return up, line, copy
 
     def arrived(chunk, slot):
         return pltpu.make_async_remote_copy(
             sbuf.at[chunk, 0], rbuf.at[chunk, slot], rs_ss.at[chunk, 0], rs_rs.at[chunk, slot], device_id={"sp": me}
         )
 
-    def reduce_chunk(chunk):
-        near = chunk == 0
+    def add_along(chunk, slot, up, line):
+        acc[...] = product(tall, line, chunk)
+        before = up * jnp.minimum(z, 1) + (1 - up) * jnp.minimum(ups, 1)
+
+        @pl.when(before == 1)
+        def _():
+            arrived(chunk, line).wait_recv()
+            sbuf[chunk, slot] = (acc[...] + rbuf[chunk, line].astype(F32)).astype(BF16)
+
+        @pl.when(before == 0)
+        def _():
+            sbuf[chunk, slot] = acc[...].astype(BF16)
+
+        hop(chunk, slot, up, line).start()
+
+    def inward(end_chunk, mid_chunk):
+        end_runs, mid_runs = int(end_chunk < chunks), int(0 <= mid_chunk < chunks)
+        runs = end_here * end_runs + (1 - end_here) * mid_runs
+        chunk = end_here * end_chunk + (1 - end_here) * mid_chunk
+
+        @pl.when(runs == 1)
+        def _():
+            w_take(chunk).wait_recv()
 
         def one(k, c):
-            up, line, copy = hop(chunk, k, near)
-            acc[...] = product(tall, line, chunk)
-            before = up * jnp.minimum(z, 1) + (1 - up) * jnp.minimum(ups, 1)
-
-            @pl.when(before == 1)
-            def _():
-                arrived(chunk, line).wait_recv()
-                sbuf[chunk, k] = (acc[...] + rbuf[chunk, line].astype(F32)).astype(BF16)
-
-            @pl.when(before == 0)
-            def _():
-                sbuf[chunk, k] = acc[...].astype(BF16)
-
-            copy.start()
+            line = inner_up * (lines - 1 - k) + (1 - inner_up) * k
+            add_along(chunk, k, inner_up, line)
             return c
 
-        w_take(chunk).wait_recv()
-        lax.fori_loop(0, lines - 1, one, 0)
+        lax.fori_loop(0, runs * inner_count, one, 0)
+
+    def outward(chunk):
+        def one(k, c):
+            line = (1 - inner_up) * (lines - 1 - k) + inner_up * k
+            add_along(chunk, inner_count + k, 1 - inner_up, line)
+            return c
+
+        lax.fori_loop(0, lines - 1 - inner_count, one, 0)
 
     def own_chunk(chunk):
         acc[...] = product(nbuf, z, chunk)
@@ -817,11 +857,17 @@
 
         proj[chunk] = acc[...].astype(BF16)
 
-    reduce_chunk(0)
-    reduce_chunk(1)
-    wo_inward(False)
+    inward(0, -1)
+    inward(1, -1)
+    inward(2, 0)
+    wo_first((0,))
+    wo_second(True, False)
+    inward(3, 1)
+    wo_first(range(1, WO_PIECES))
+    outward(0)
     own_chunk(0)
-    reduce_chunk(2)
+    inward(4, 2)
+    outward(1)
     own_chunk(1)
 
     keys_f = proj[0, :, dk:].astype(F32)
@@ -841,21 +887,32 @@
         pack_out[d, 2:3, :] = jnp.broadcast_to(stable, (1, wide))
         pack_out[d, 3:, :] = jnp.zeros((5, wide), F32)
 
+    def swap_states():
+        return (
+            pltpu.make_async_remote_copy(state_out, mate_state, st_ss.at[lines], st_rs.at[lines], device_id={"sp": mate}),
+            pltpu.make_async_remote_copy(pack_out, mate_pack, pk_ss.at[lines], pk_rs.at[lines], device_id={"sp": mate}),
+        )
+
+    for copy in swap_states():
+        copy.start()
+    wo_second(False, True)
+    wo_rest(2, (0,))
+
     def give(o):
-        other = lax.rem(me + o, n)
-        d = lax.div(me + o, n)
-        ids = {"sp": other}
+        other = lax.rem(z + o, lines)
+        d = lax.div(z + o, lines)
+        ids = {"sp": at_line(other)}
         return (
-            pltpu.make_async_remote_copy(state_out.at[d], state_in.at[me], st_ss.at[o], st_rs.at[me], device_id=ids),
-            pltpu.make_async_remote_copy(pack_out.at[d], pack_in.at[me], pk_ss.at[o], pk_rs.at[me], device_id=ids),
+            pltpu.make_async_remote_copy(pair_state.at[d], state_in.at[z], st_ss.at[o], st_rs.at[z], device_id=ids),
+            pltpu.make_async_remote_copy(pair_pack.at[d], pack_in.at[z], pk_ss.at[o], pk_rs.at[z], device_id=ids),
         )
 
     def take(o):
-        source = lax.rem(me + o, n)
-        ids = {"sp": source}
+        source = lax.rem(z + o, lines)
+        ids = {"sp": at_line(source)}
         return (
-            pltpu.make_async_remote_copy(state_out.at[0], state_in.at[source], st_ss.at[o], st_rs.at[source], device_id=ids),
-            pltpu.make_async_remote_copy(pack_out.at[0], pack_in.at[source], pk_ss.at[o], pk_rs.at[source], device_id=ids),
+            pltpu.make_async_remote_copy(pair_state.at[0], state_in.at[source], st_ss.at[o], st_rs.at[source], device_id=ids),
+            pltpu.make_async_remote_copy(pair_pack.at[0], pack_in.at[source], pk_ss.at[o], pk_rs.at[source], device_id=ids),
         )
 
     def give_all(o, c):
@@ -873,9 +930,36 @@
             copy.wait_send()
         return c
 
-    lax.fori_loop(1, n, give_all, 0)
-
-    reduce_chunk(3)
+    def blend(first, second):
+        total = first[1:2, :] + second[1:2, :]
+        moved = first[2:3, :] + second[1:2, :]
+        stable = jnp.maximum(moved, second[2:3, :])
+        return total, stable, jnp.exp(moved - stable), jnp.exp(second[2:3, :] - stable)
+
+    def pair_up():
+        for copy in swap_states():
+            copy.wait_recv()
+        own_first = (1 - y).astype(F32)
+        for d in range(2):
+            lead = own_first if d == 0 else 1.0 - own_first
+            mine_p, other_p = pack_out[d], mate_pack[d]
+            first = lead * mine_p + (1.0 - lead) * other_p
+            second = lead * other_p + (1.0 - lead) * mine_p
+            total, stable, first_w, second_w = blend(first, second)
+            mine_w = lead * first_w + (1.0 - lead) * second_w
+            other_w = lead * second_w + (1.0 - lead) * first_w
+            joint = mine_w * state_out[d].astype(F32) + other_w * mate_state[d].astype(F32)
+            pair_state[d] = joint.astype(BF16)
+            pair_pack[d, 0:1, :] = mine_w * mine_p[0:1, :] + other_w * other_p[0:1, :]
+            pair_pack[d, 1:2, :] = total
+            pair_pack[d, 2:3, :] = stable
+            pair_pack[d, 3:, :] = jnp.zeros((5, wide), F32)
+
+    inward(5, 3)
+    pair_up()
+    lax.fori_loop(1, lines, give_all, 0)
+    outward(2)
+    wo_rest(2, range(1, WO_PIECES))
     own_chunk(2)
 
     scale = dk ** (-0.5)
@@ -892,8 +976,8 @@
         local_num[d] = dot(part.astype(BF16), proj[1], NN)
         local.append((cum_c, peak, jnp.sum(part, axis=-1, keepdims=True)))
 
-    reduce_chunk(4)
-    wo_inward(True)
+    inward(6, 4)
+    outward(3)
     own_chunk(3)
 
     mixed = (proj[2].astype(F32) * proj[3].astype(F32)).astype(BF16).astype(F32)
@@ -918,8 +1002,9 @@
     def _():
         edge(1).start()
 
-    for line in range(1, lines - 1):
-        wo_relay(line)
+    for away in range(3, lines):
+        wo_rest(away, range(WO_PIECES))
+    outward(4)
 
     def share(part, o, source):
         columns = pl.ds(part * dv, dv)
@@ -932,25 +1017,32 @@
             device_id={"tp": lax.rem(head + o, t)},
         )
 
-    lax.fori_loop(1, n, take_all, 0)
+    lax.fori_loop(1, lines, take_all, 0)
     summed = None
     query_f = proj[0, :, :dk].astype(F32) * scale
     for d in range(2):
         carry_c[...] = jnp.zeros_like(carry_c)
         carry_n[...] = jnp.zeros_like(carry_n)
 
-        def join(i, peak_in):
-            source = i if d == 0 else n - 1 - i
-            total = pack_in[source, 1:2, :]
-            stable = pack_in[source, 2:3, :]
+        def merge(state, pack, peak_in):
+            total = pack[1:2, :]
+            stable = pack[2:3, :]
             new = jnp.maximum(peak_in + total, stable)
             old_w = jnp.exp(peak_in + total - new)
             new_w = jnp.exp(stable - new)
-            carry_c[...] = old_w * carry_c[...] + new_w * state_in[source].astype(F32)
-            carry_n[...] = old_w * carry_n[...] + new_w * pack_in[source, 0:1, :]
+            carry_c[...] = old_w * carry_c[...] + new_w * state.astype(F32)
+            carry_n[...] = old_w * carry_n[...] + new_w * pack[0:1, :]
             return new
 
-        peak_in = lax.fori_loop(0, me if d == 0 else n - 1 - me, join, jnp.full((1, dv), LOWEST, F32))
+        def join(i, peak_in):
+            source = i if d == 0 else lines - 1 - i
+            return merge(state_in[source], pack_in[source], peak_in)
+
+        def join_mate(i, peak_in):
+            return merge(mate_state[d], mate_pack[d], peak_in)
+
+        peak_in = lax.fori_loop(0, z if d == 0 else ups, join, jnp.full((1, dv), LOWEST, F32))
+        peak_in = lax.fori_loop(0, y if d == 0 else 1 - y, join_mate, peak_in)
         cum_c, peak, den = local[d]
         carried = cum_c + peak_in[:, :1]
         top = jnp.maximum(carried, peak)
@@ -985,9 +1077,6 @@
     for o in range(1, t):
         share(1, o, head).start()
 
-    wo_relay(0)
-    wo_relay(lines - 1)
-
     for line in range(lines):
         for piece in range(WO_PIECES):
             wo_mate_take(line, piece).wait_recv()
@@ -1013,14 +1102,20 @@
         token_send(line).wait_send()
         for way in range(3):
             token_pass(line, way).wait_send()
+        inner = jnp.clip(inner_count - k, 0, 1)
+        up = inner * inner_up + (1 - inner) * (1 - inner_up)
+        step = inner * k + (1 - inner) * (k - inner_count)
+        line = up * (lines - 1 - step) + (1 - up) * step
         for chunk in range(chunks):
-            hop(chunk, k, chunk == 0)[2].wait_send()
+            hop(chunk, k, up, line).wait_send()
         return c
 
     lax.fori_loop(0, lines - 1, token_end, 0)
     for chunk in range(chunks):
         w_send(chunk).wait_send()
-    lax.fori_loop(1, n, give_end, 0)
+    for copy in swap_states():
+        copy.wait_send()
+    lax.fori_loop(1, lines, give_end, 0)
 
     @pl.when(later_exists)
     def _():
@@ -1106,8 +1201,12 @@
             pltpu.VMEM((8, rows), F32),
             pltpu.VMEM((2, dk, dv), BF16),
             pltpu.VMEM((2, 8, dv), F32),
-            pltpu.VMEM((n, dk, dv), BF16),
-            pltpu.VMEM((n, 8, dv), F32),
+            pltpu.VMEM((2, dk, dv), BF16),
+            pltpu.VMEM((2, 8, dv), F32),
+            pltpu.VMEM((2, dk, dv), BF16),
+            pltpu.VMEM((2, 8, dv), F32),
+            pltpu.VMEM((lines, dk, dv), BF16),
+            pltpu.VMEM((lines, 8, dv), F32),
             pltpu.VMEM((2, 8, dv), F32),
             pltpu.VMEM((2, 8, dv), F32),
             pltpu.VMEM((dk, dv), F32),
@@ -1123,10 +1222,10 @@
             dma((chunks,)),
             dma((chunks, lines - 1)),
             dma((chunks, lines + 1)),
-            dma((n,)),
-            dma((n,)),
-            dma((n,)),
-            dma((n,)),
+            dma((lines + 1,)),
+            dma((lines + 1,)),
+            dma((lines + 1,)),
+            dma((lines + 1,)),
             dma((2,)),
             dma((2,)),
             dma((2, t)),

time: 146 us -> 97.2 us (0.67)
  Pallas kernels: 144 us -> 94.4 us
    pallas_call x1, Pallas kernels: 144 us -> 94.4 us  [body(): pl.pallas_call(functools.partial(kernel, n, t, dk, dv), out_shape=jax.Sha...]
where the time goes in v2:
time: 97.2 us; the launch traced here: 96.2 us
  Pallas kernels  94.4 us (97%)
  local copies, waits for them, and re-layouts  1.87 us (2%)
    pallas_call x1, Pallas kernels, body(): pl.pallas_call(functools.partial(kernel, n, t, dk, dv), out_shape=jax.Sha...  94.4 us

profile of v2, /device:TPU:0, one launch (start us, length us, event | category | flops | bytes accessed | tf_op | source)
XLA Modules:
  0.0 96.2 jit_solution(1027952622005944252)
XLA Ops:
  0.0 94.4 %shard_map.145 = bf16[256,1024]{1,0:T(8,128)(2,1)} custom-call(bf16[256,4096]{1,0:T(8,128)(2,1)} %tokens.1, f32[1,4096]{1,0:T(1,128)} %bitcast.9, bf16[512,128]{1,0:T(8,128)(2,1)} %w_query.1, bf16[512,128]{1,0:T(8,128)(2,1)} %w_key.1, bf16[512,256]{1,0:T(8,128)(2,1)} %w_value.1, bf16[512,256]{1,0:T(8,128)(2,1)} %w_conv_b.1, bf16[512,256]{1,0:T(8,128)(2,1)} %w_conv_c.1, ...), custom_call_target="tpu_custom_call" | custom-call | tf_op jit(solution)/shard_map/pallas_call | solution.py:1185
  94.4 1.9 %copy.17 = bf16[256,1024]{1,0:T(8,128)(2,1)} copy(bf16[256,1024]{1,0:T(8,128)(2,1)} %shard_map.145) | data formatting | bytes 1048576

commit v3 on v2

--- a/solution.py
+++ b/solution.py
@@ -517,6 +517,7 @@
     local_num,
     joined,
     own_sem,
+    tok_sem,
     tk_ss,
     tk_rs,
     tf_ss,
@@ -533,6 +534,8 @@
     ed_rs,
     j_ss,
     j_rs,
+    jp_ss,
+    jp_rs,
     oz_ss,
     oz_rs,
     oy_ss,
@@ -556,8 +559,17 @@
     def at_line(line):
         return PAIR * line + y
 
-    load_tok = pltpu.make_async_copy(tokens, tok, own_sem.at[0])
-    load_tok.start()
+    rows_at_once = 32
+
+    def load_rows(i):
+        span = pl.ds(pl.multiple_of(i * rows_at_once, rows_at_once), rows_at_once)
+        return pltpu.make_async_copy(tokens.at[span, :], tok.at[span, :], tok_sem.at[i])
+
+    def load_start(i, c):
+        load_rows(i).start()
+        return c
+
+    lax.fori_loop(0, rows // rows_at_once, load_start, 0)
     mine = pl.ds(pl.multiple_of(y * depth, depth), depth)
     loads = []
     plan = ((w_query, 0, 0), (w_key, 0, dk), (w_value, 1, 0), (w_conv_c, 2, 0), (w_conv_in, 3, 0), (w_conv_b, 4, 0))
@@ -585,10 +597,8 @@
     lax.fori_loop(1, n, greet_sp, 0)
     lax.fori_loop(1, t, greet_tp, 0)
 
-    load_tok.wait()
-    rows_at_once = 32
-
     def norm_rows(i, c):
+        load_rows(i).wait()
         span = pl.ds(pl.multiple_of(i * rows_at_once, rows_at_once), rows_at_once)
         values = tok[span, :].astype(F32)
         inverse = lax.rsqrt(jnp.mean(values * values, axis=-1, keepdims=True) + EPS)
@@ -720,15 +730,15 @@
 
     inner_way = 2 * inner_up - 1
 
-    def wo_first(pieces_now):
-        wo_relay(z - inner_way * (1 - 2 * end_here), True, True, True, pieces_now)
+    def wo_first(pieces_now, along=True, across=True, wanted=True):
+        wo_relay(z - inner_way * (1 - 2 * end_here), wanted, along, across, pieces_now)
 
     def wo_second(along, across):
         wo_relay(z + inner_way, jnp.logical_not(at_end), along, across)
 
-    def wo_rest(away, pieces_now):
-        wo_relay(z - away, True, True, True, pieces_now)
-        wo_relay(z + away, True, True, True, pieces_now)
+    def wo_rest(away, pieces_now, along=True, across=True, wanted=True):
+        wo_relay(z - away, wanted, along, across, pieces_now)
+        wo_relay(z + away, wanted, along, across, pieces_now)
 
     for piece in range(WO_PIECES):
         wo_mate(z, piece).start()
@@ -781,80 +791,106 @@
     wo_inward(False)
     lax.fori_loop(0, lines - 1, relay_across, 0)
     lax.fori_loop(0, lines - 1, tokens_ready, 0)
-    def product(source, line, chunk):
-        total = dot(source[line, 0], wbuf[chunk, 0:part_k, :], NN)
-        for q in range(1, t):
-            total += dot(source[line, q], wbuf[chunk, q * part_k : (q + 1) * part_k, :], NN)
-        return total
-
-    def hop(chunk, k, up, line):
+    def parts_of(chunk):
+        if isinstance(chunk, int) and chunk == chunks - 1:
+            return ((0, rows // 2, chunk), (rows // 2, rows // 2, chunks))
+        return ((0, rows, chunk),)
+
+    def hop(chunk, part, k, up, line):
+        first, count, sem = part
         last = (1 - up) * (1 - jnp.minimum(jnp.abs(z - line) - 1, 1))
         slot = line + last * (lines - line)
         return pltpu.make_async_remote_copy(
-            sbuf.at[chunk, k],
-            rbuf.at[chunk, slot],
-            rs_ss.at[chunk, k],
-            rs_rs.at[chunk, slot],
+            sbuf.at[chunk, k, pl.ds(first, count)],
+            rbuf.at[chunk, slot, pl.ds(first, count)],
+            rs_ss.at[sem, k],
+            rs_rs.at[sem, slot],
             device_id={"sp": at_line(z + 2 * up - 1)},
         )
 
-    def arrived(chunk, slot):
+    def arrived(chunk, part, slot):
+        first, count, sem = part
         return pltpu.make_async_remote_copy(
-            sbuf.at[chunk, 0], rbuf.at[chunk, slot], rs_ss.at[chunk, 0], rs_rs.at[chunk, slot], device_id={"sp": me}
-        )
-
-    def add_along(chunk, slot, up, line):
-        acc[...] = product(tall, line, chunk)
+            sbuf.at[chunk, 0, pl.ds(first, count)],
+            rbuf.at[chunk, slot, pl.ds(first, count)],
+            rs_ss.at[sem, 0],
+            rs_rs.at[sem, slot],
+            device_id={"sp": me},
+        )
+
+    def product(source, line, chunk, part):
+        span = pl.ds(part[0], part[1])
+        total = dot(source[line, 0, span, :], wbuf[chunk, 0:part_k, :], NN)
+        for q in range(1, t):
+            total += dot(source[line, q, span, :], wbuf[chunk, q * part_k : (q + 1) * part_k, :], NN)
+        return total
+
+    def add_along(chunk, part, slot, up, line):
+        span = pl.ds(part[0], part[1])
+        acc[span, :] = product(tall, line, chunk, part)
         before = up * jnp.minimum(z, 1) + (1 - up) * jnp.minimum(ups, 1)
 
         @pl.when(before == 1)
         def _():
-            arrived(chunk, line).wait_recv()
-            sbuf[chunk, slot] = (acc[...] + rbuf[chunk, line].astype(F32)).astype(BF16)
+            arrived(chunk, part, line).wait_recv()
+            sbuf[chunk, slot, span, :] = (acc[span, :] + rbuf[chunk, line, span, :].astype(F32)).astype(BF16)
 
         @pl.when(before == 0)
         def _():
-            sbuf[chunk, slot] = acc[...].astype(BF16)
-
-        hop(chunk, slot, up, line).start()
-
-    def inward(end_chunk, mid_chunk):
-        end_runs, mid_runs = int(end_chunk < chunks), int(0 <= mid_chunk < chunks)
-        runs = end_here * end_runs + (1 - end_here) * mid_runs
-        chunk = end_here * end_chunk + (1 - end_here) * mid_chunk
-
+            sbuf[chunk, slot, span, :] = acc[span, :].astype(BF16)
+
+        hop(chunk, part, slot, up, line).start()
+
+    def inward_where(runs, chunk):
         @pl.when(runs == 1)
         def _():
             w_take(chunk).wait_recv()
 
-        def one(k, c):
-            line = inner_up * (lines - 1 - k) + (1 - inner_up) * k
-            add_along(chunk, k, inner_up, line)
-            return c
-
-        lax.fori_loop(0, runs * inner_count, one, 0)
+        for part in parts_of(chunk):
+
+            def one(k, c):
+                line = inner_up * (lines - 1 - k) + (1 - inner_up) * k
+                add_along(chunk, part, k, inner_up, line)
+                return c
+
+            lax.fori_loop(0, runs * inner_count, one, 0)
+
+    def inward(end_chunk, mid_chunk):
+        end_runs, mid_runs = end_chunk < chunks, mid_chunk >= 0
+        if end_runs and mid_runs and max(end_chunk, mid_chunk) < chunks - 1:
+            inward_where(1, end_here * end_chunk + (1 - end_here) * mid_chunk)
+            return
+        if end_runs:
+            inward_where(end_here, end_chunk)
+        if mid_runs:
+            inward_where(1 - end_here, mid_chunk)
 
     def outward(chunk):
-        def one(k, c):
-            line = (1 - inner_up) * (lines - 1 - k) + inner_up * k
-            add_along(chunk, inner_count + k, 1 - inner_up, line)
-            return c
-
-        lax.fori_loop(0, lines - 1 - inner_count, one, 0)
-
-    def own_chunk(chunk):
-        acc[...] = product(nbuf, z, chunk)
+        for part in parts_of(chunk):
+
+            def one(k, c):
+                line = (1 - inner_up) * (lines - 1 - k) + inner_up * k
+                add_along(chunk, part, inner_count + k, 1 - inner_up, line)
+                return c
+
+            lax.fori_loop(0, lines - 1 - inner_count, one, 0)
+
+    def own_part(chunk, part):
+        span = pl.ds(part[0], part[1])
+        acc[span, :] = product(nbuf, z, chunk, part)
 
         @pl.when(has_down)
         def _():
-            arrived(chunk, z).wait_recv()
-            acc[...] += rbuf[chunk, z].astype(F32)
+            arrived(chunk, part, z).wait_recv()
+            acc[span, :] += rbuf[chunk, z, span, :].astype(F32)
 
         @pl.when(has_up)
         def _():
-            arrived(chunk, lines).wait_recv()
-            acc[...] += rbuf[chunk, lines].astype(F32)
-
+            arrived(chunk, part, lines).wait_recv()
+            acc[span, :] += rbuf[chunk, lines, span, :].astype(F32)
+
+    def own_chunk(chunk):
+        own_part(chunk, parts_of(chunk)[0])
         proj[chunk] = acc[...].astype(BF16)
 
     inward(0, -1)
@@ -863,10 +899,11 @@
     wo_first((0,))
     wo_second(True, False)
     inward(3, 1)
-    wo_first(range(1, WO_PIECES))
+    wo_first(range(1, WO_PIECES), True, False)
+    wo_first(range(1, WO_PIECES), False, True, at_end)
     outward(0)
     own_chunk(0)
-    inward(4, 2)
+    inward(chunks, 2)
     outward(1)
     own_chunk(1)
 
@@ -889,46 +926,61 @@
 
     def swap_states():
         return (
-            pltpu.make_async_remote_copy(state_out, mate_state, st_ss.at[lines], st_rs.at[lines], device_id={"sp": mate}),
-            pltpu.make_async_remote_copy(pack_out, mate_pack, pk_ss.at[lines], pk_rs.at[lines], device_id={"sp": mate}),
+            pltpu.make_async_remote_copy(state_out, mate_state, st_ss.at[2], st_rs.at[2], device_id={"sp": mate}),
+            pltpu.make_async_remote_copy(pack_out, mate_pack, pk_ss.at[2], pk_rs.at[2], device_id={"sp": mate}),
         )
 
     for copy in swap_states():
         copy.start()
+    wo_first(range(1, WO_PIECES), False, True, jnp.logical_not(at_end))
     wo_second(False, True)
-    wo_rest(2, (0,))
-
-    def give(o):
-        other = lax.rem(z + o, lines)
-        d = lax.div(z + o, lines)
-        ids = {"sp": at_line(other)}
+    wo_rest(2, (0,), True, True)
+    wo_rest(2, range(1, WO_PIECES), True, False)
+    wo_rest(2, range(1, WO_PIECES), False, True, at_end)
+
+    d_in, d_out = 1 - inner_up, inner_up
+
+    def chain(d, way):
+        ids = {"sp": at_line(z + way)}
         return (
-            pltpu.make_async_remote_copy(pair_state.at[d], state_in.at[z], st_ss.at[o], st_rs.at[z], device_id=ids),
-            pltpu.make_async_remote_copy(pair_pack.at[d], pack_in.at[z], pk_ss.at[o], pk_rs.at[z], device_id=ids),
-        )
-
-    def take(o):
-        source = lax.rem(z + o, lines)
-        ids = {"sp": at_line(source)}
-        return (
-            pltpu.make_async_remote_copy(pair_state.at[0], state_in.at[source], st_ss.at[o], st_rs.at[source], device_id=ids),
-            pltpu.make_async_remote_copy(pair_pack.at[0], pack_in.at[source], pk_ss.at[o], pk_rs.at[source], device_id=ids),
-        )
-
-    def give_all(o, c):
-        for copy in give(o):
-            copy.start()
-        return c
-
-    def take_all(o, c):
-        for copy in take(o):
+            pltpu.make_async_remote_copy(pair_state.at[d], state_in.at[d], st_ss.at[d], st_rs.at[d], device_id=ids),
+            pltpu.make_async_remote_copy(pair_pack.at[d], pack_in.at[d], pk_ss.at[d], pk_rs.at[d], device_id=ids),
+        )
+
+    def chain_add(d):
+        for copy in chain(d, 0):
             copy.wait_recv()
-        return c
-
-    def give_end(o, c):
-        for copy in give(o):
-            copy.wait_send()
-        return c
+        total, stable, first_w, second_w = blend(pack_in[d], pair_pack[d])
+        joint = first_w[:, :1] * state_in[d].astype(F32) + second_w[:, :1] * pair_state[d].astype(F32)
+        pair_state[d] = joint.astype(BF16)
+        pair_pack[d, 0:1, :] = first_w * pack_in[d, 0:1, :] + second_w * pair_pack[d, 0:1, :]
+        pair_pack[d, 1:2, :] = total
+        pair_pack[d, 2:3, :] = stable
+
+    def chain_from_end():
+        @pl.when(at_end)
+        def _():
+            for copy in chain(d_in, inner_way):
+                copy.start()
+
+    def chain_inward():
+        @pl.when(jnp.logical_not(at_end))
+        def _():
+            chain_add(d_in)
+            for copy in chain(d_in, inner_way):
+                copy.start()
+
+    def chain_outward():
+        @pl.when(jnp.logical_not(at_end))
+        def _():
+            chain_add(d_out)
+            for copy in chain(d_out, -inner_way):
+                copy.start()
+
+        @pl.when(at_end)
+        def _():
+            for copy in chain(d_out, 0):
+                copy.wait_recv()
 
     def blend(first, second):
         total = first[1:2, :] + second[1:2, :]
@@ -955,11 +1007,13 @@
             pair_pack[d, 2:3, :] = stable
             pair_pack[d, 3:, :] = jnp.zeros((5, wide), F32)
 
-    inward(5, 3)
+    inward(chunks, 3)
     pair_up()
-    lax.fori_loop(1, lines, give_all, 0)
+    chain_from_end()
+    inward(4, -1)
     outward(2)
-    wo_rest(2, range(1, WO_PIECES))
+    for away in range(3, lines):
+        wo_rest(away, (0,))
     own_chunk(2)
 
     scale = dk ** (-0.5)
@@ -976,7 +1030,8 @@
         local_num[d] = dot(part.astype(BF16), proj[1], NN)
         local.append((cum_c, peak, jnp.sum(part, axis=-1, keepdims=True)))
 
-    inward(6, 4)
+    chain_inward()
+    inward(chunks, 4)
     outward(3)
     own_chunk(3)
 
@@ -1002,22 +1057,54 @@
     def _():
         edge(1).start()
 
+    wo_rest(2, range(1, WO_PIECES), False, True, jnp.logical_not(at_end))
     for away in range(3, lines):
-        wo_rest(away, range(WO_PIECES))
+        wo_rest(away, range(1, WO_PIECES))
+    chain_outward()
     outward(4)
 
-    def share(part, o, source):
+    half_rows = rows // 2
+
+    def joined_part(part, source, way):
         columns = pl.ds(part * dv, dv)
-        slot = joined.at[source, :, columns]
+        if way == 0:
+            return joined.at[source, :, columns]
+        return joined.at[source, pl.ds((way - 1) * half_rows, half_rows), columns]
+
+    others = (core_mate, x_mate, far_mate)
+
+    def share(part, way, source):
+        slot = joined_part(part, source, way)
         return pltpu.make_async_remote_copy(
-            slot,
-            slot,
-            j_ss.at[part, o],
-            j_rs.at[part, source],
-            device_id={"tp": lax.rem(head + o, t)},
-        )
-
-    lax.fori_loop(1, lines, take_all, 0)
+            slot, slot, j_ss.at[part, way], j_rs.at[part, way], device_id={"tp": others[way]}
+        )
+
+    def share_pass(part, way, source):
+        slot = joined_part(part, source, way)
+        return pltpu.make_async_remote_copy(
+            slot, slot, jp_ss.at[part, way - 1], jp_rs.at[part, way - 1], device_id={"tp": core_mate}
+        )
+
+    def share_start(part):
+        for way in (1, 2, 0):
+            share(part, way, head).start()
+
+    def share_relay(part):
+        for way in (1, 2):
+            share(part, way, others[way]).wait_recv()
+            share_pass(part, way, others[way]).start()
+
+    def share_wait(part):
+        share(part, 0, core_mate).wait_recv()
+        for way in (1, 2):
+            share_pass(part, way, others[3 - way]).wait_recv()
+
+    def share_end(part):
+        for way in range(3):
+            share(part, way, head).wait_send()
+        for way in (1, 2):
+            share_pass(part, way, others[way]).wait_send()
+
     summed = None
     query_f = proj[0, :, :dk].astype(F32) * scale
     for d in range(2):
@@ -1035,13 +1122,12 @@
             return new
 
         def join(i, peak_in):
-            source = i if d == 0 else lines - 1 - i
-            return merge(state_in[source], pack_in[source], peak_in)
+            return merge(state_in[d], pack_in[d], peak_in)
 
         def join_mate(i, peak_in):
             return merge(mate_state[d], mate_pack[d], peak_in)
 
-        peak_in = lax.fori_loop(0, z if d == 0 else ups, join, jnp.full((1, dv), LOWEST, F32))
+        peak_in = lax.fori_loop(0, jnp.minimum(z if d == 0 else ups, 1), join, jnp.full((1, dv), LOWEST, F32))
         peak_in = lax.fori_loop(0, y if d == 0 else 1 - y, join_mate, peak_in)
         cum_c, peak, den = local[d]
         carried = cum_c + peak_in[:, :1]
@@ -1054,10 +1140,7 @@
         summed = result if d == 0 else summed + result
     inverse = lax.rsqrt(jnp.mean(summed * summed, axis=-1, keepdims=True) + EPS)
     joined[head, :, :dv] = (summed * inverse * head_gain[...]).astype(BF16)
-    for o in range(1, t):
-        share(0, o, head).start()
-
-    own_chunk(4)
+    share_start(0)
 
     @pl.when(prior_exists)
     def _():
@@ -1072,17 +1155,22 @@
     prior = jnp.where(pos == 0, edge_in[0, 0:1, :], pltpu.roll(mixed, 1, 0))
     later = jnp.where(pos == rows - 1, edge_in[1, 0:1, :], pltpu.roll(mixed, rows - 1, 0))
     taps_f = taps[...].astype(F32)
-    filtered = taps_f[0:1] * prior + taps_f[1:2] * mixed + taps_f[2:3] * later
-    joined[head, :, dv:] = (proj[4].astype(F32) * filtered).astype(BF16)
-    for o in range(1, t):
-        share(1, o, head).start()
+    local_num[0] = taps_f[0:1] * prior + taps_f[1:2] * mixed + taps_f[2:3] * later
+    for i, part in enumerate(parts_of(chunks - 1)):
+        span = pl.ds(part[0], part[1])
+        own_part(chunks - 1, part)
+        outer = acc[span, :].astype(BF16).astype(F32)
+        joined[head, span, dv:] = (outer * local_num[0, span, :]).astype(BF16)
+        share(1, 1 + i, head).start()
+    share(1, 0, head).start()
+    share_relay(0)
+    share_relay(1)
 
     for line in range(lines):
         for piece in range(WO_PIECES):
             wo_mate_take(line, piece).wait_recv()
     for part in range(2):
-        for o in range(1, t):
-            share(part, o, lax.rem(head + o, t)).wait_recv()
+        share_wait(part)
 
     span_j = 2 * dv
     width = 256
@@ -1107,7 +1195,8 @@
         step = inner * k + (1 - inner) * (k - inner_count)
         line = up * (lines - 1 - step) + (1 - up) * step
         for chunk in range(chunks):
-            hop(chunk, k, up, line).wait_send()
+            for part in parts_of(chunk):
+                hop(chunk, part, k, up, line).wait_send()
         return c
 
     lax.fori_loop(0, lines - 1, token_end, 0)
@@ -1115,7 +1204,17 @@
         w_send(chunk).wait_send()
     for copy in swap_states():
         copy.wait_send()
-    lax.fori_loop(1, lines, give_end, 0)
+
+    @pl.when(at_end)
+    def _():
+        for copy in chain(d_in, inner_way):
+            copy.wait_send()
+
+    @pl.when(jnp.logical_not(at_end))
+    def _():
+        for copy in chain(d_in, inner_way) + chain(d_out, -inner_way):
+            copy.wait_send()
+
 
     @pl.when(later_exists)
     def _():
@@ -1126,8 +1225,7 @@
         edge(1).wait_send()
 
     for part in range(2):
-        for o in range(1, t):
-            share(part, o, head).wait_send()
+        share_end(part)
     for piece in range(WO_PIECES):
 
         @pl.when(has_up)
@@ -1205,8 +1303,8 @@
             pltpu.VMEM((2, 8, dv), F32),
             pltpu.VMEM((2, dk, dv), BF16),
             pltpu.VMEM((2, 8, dv), F32),
-            pltpu.VMEM((lines, dk, dv), BF16),
-            pltpu.VMEM((lines, 8, dv), F32),
+            pltpu.VMEM((2, dk, dv), BF16),
+            pltpu.VMEM((2, 8, dv), F32),
             pltpu.VMEM((2, 8, dv), F32),
             pltpu.VMEM((2, 8, dv), F32),
             pltpu.VMEM((dk, dv), F32),
@@ -1214,22 +1312,25 @@
             pltpu.VMEM((2, rows, dv), F32),
             pltpu.VMEM((t, rows, 2 * dv), BF16),
             dma((8,)),
+            dma((rows // 32,)),
             dma((lines,)),
             dma((lines,)),
             dma((3, lines)),
             dma((3, lines)),
             dma((chunks,)),
             dma((chunks,)),
-            dma((chunks, lines - 1)),
-            dma((chunks, lines + 1)),
-            dma((lines + 1,)),
-            dma((lines + 1,)),
-            dma((lines + 1,)),
-            dma((lines + 1,)),
+            dma((chunks + 1, lines - 1)),
+            dma((chunks + 1, lines + 1)),
+            dma((3,)),
+            dma((3,)),
+            dma((3,)),
+            dma((3,)),
             dma((2,)),
             dma((2,)),
-            dma((2, t)),
-            dma((2, t)),
+            dma((2, 3)),
+            dma((2, 3)),
+            dma((2, 2)),
+            dma((2, 2)),
             dma((lines + 2, WO_PIECES)),
             dma((lines, WO_PIECES)),
             dma((lines, WO_PIECES)),

time: 97.2 us -> 93.6 us (0.963)
  Pallas kernels: 94.4 us -> 90.8 us
    pallas_call x1, Pallas kernels: 94.4 us -> 90.8 us  [body(): pl.pallas_call(functools.partial(kernel, n, t, dk, dv), out_shape=jax.Sha...]
where the time goes in v3:
time: 93.6 us; the launch traced here: 92.6 us
  Pallas kernels  90.8 us (97%)
  local copies, waits for them, and re-layouts  1.87 us (2%)
    pallas_call x1, Pallas kernels, body(): pl.pallas_call(functools.partial(kernel, n, t, dk, dv), out_shape=jax.Sha...  90.8 us

profile of v3, /device:TPU:0, one launch (start us, length us, event | category | flops | bytes accessed | tf_op | source)
XLA Modules:
  0.0 92.6 jit_solution(15702678252476895865)
XLA Ops:
  0.0 90.8 %shard_map.145 = bf16[256,1024]{1,0:T(8,128)(2,1)} custom-call(bf16[256,4096]{1,0:T(8,128)(2,1)} %tokens.1, f32[1,4096]{1,0:T(1,128)} %bitcast.9, bf16[512,128]{1,0:T(8,128)(2,1)} %w_query.1, bf16[512,128]{1,0:T(8,128)(2,1)} %w_key.1, bf16[512,256]{1,0:T(8,128)(2,1)} %w_value.1, bf16[512,256]{1,0:T(8,128)(2,1)} %w_conv_b.1, bf16[512,256]{1,0:T(8,128)(2,1)} %w_conv_c.1, ...), custom_call_target="tpu_custom_call" | custom-call | tf_op jit(solution)/shard_map/pallas_call | solution.py:1283
  90.8 1.9 %copy.17 = bf16[256,1024]{1,0:T(8,128)(2,1)} copy(bf16[256,1024]{1,0:T(8,128)(2,1)} %shard_map.145) | data formatting | bytes 1048576

commit v4 on v3

--- a/solution.py
+++ b/solution.py
@@ -516,6 +516,8 @@
     carry_n,
     local_num,
     joined,
+    result,
+    out_sem,
     own_sem,
     tok_sem,
     tk_ss,
@@ -540,6 +542,8 @@
     oz_rs,
     oy_ss,
     oy_rs,
+    ox_ss,
+    ox_rs,
 ):
     me = lax.axis_index("sp")
     head = lax.axis_index("tp")
@@ -726,15 +730,63 @@
                         wo_line(line, piece, -1, line).start()
 
                 if across:
-                    wo_mate(line, piece).start()
+
+                    @pl.when(from_mate(line, piece))
+                    def _():
+                        wo_mate(line, piece).start()
+
+                    if spread and piece == tail_piece:
+
+                        @pl.when(jnp.logical_and(at_end, line == near_line))
+                        def _():
+                            mate_cut(line, y).start()
 
     inner_way = 2 * inner_up - 1
+
+    spread = lines == 4
+    tail_piece = WO_PIECES - 1
+    near_line, far_line = z + inner_way, z + 2 * inner_way
+    at_mid = jnp.logical_not(at_end)
+
+    def cut_rows(index, half, halves):
+        count = tall_o // halves
+        first = index * depth_o + tail_piece * tall_o + half * count
+        return wo_all.at[pl.ds(pl.multiple_of(first, count), count), :]
+
+    def mate_cut(line, row):
+        there = cut_rows(PAIR * line + row, 1, 2)
+        return pltpu.make_async_remote_copy(
+            there, there, oy_ss.at[line, tail_piece], oy_rs.at[line, tail_piece], device_id={"sp": mate}
+        )
+
+    def along_row(line, way, kind):
+        there = cut_rows(PAIR * line + 1 - y, 0, 1 + kind)
+        return pltpu.make_async_remote_copy(
+            there, there, ox_ss.at[kind], ox_rs.at[kind], device_id={"sp": at_line(z + way)}
+        )
+
+    def from_mate(line, piece):
+        if not spread or piece != tail_piece:
+            return line >= 0
+        return jnp.logical_or(
+            jnp.logical_and(at_mid, line != far_line), jnp.logical_and(at_end, line != near_line)
+        )
+
+    def spread_send():
+        if spread:
+
+            @pl.when(at_mid)
+            def _():
+                wo_mate_take(z, tail_piece).wait_recv()
+                along_row(z, -inner_way, 1).start()
+                wo_mate_take(z - inner_way, tail_piece).wait_recv()
+                along_row(z - inner_way, inner_way, 0).start()
 
     def wo_first(pieces_now, along=True, across=True, wanted=True):
         wo_relay(z - inner_way * (1 - 2 * end_here), wanted, along, across, pieces_now)
 
-    def wo_second(along, across):
-        wo_relay(z + inner_way, jnp.logical_not(at_end), along, across)
+    def wo_second(along, across, pieces_now=range(WO_PIECES)):
+        wo_relay(z + inner_way, jnp.logical_not(at_end), along, across, pieces_now)
 
     def wo_rest(away, pieces_now, along=True, across=True, wanted=True):
         wo_relay(z - away, wanted, along, across, pieces_now)
@@ -841,19 +893,21 @@
 
         hop(chunk, part, slot, up, line).start()
 
+    def inward_span(first, last, chunk):
+        def one(k, c):
+            line = inner_up * (lines - 1 - k) + (1 - inner_up) * k
+            for part in parts_of(chunk):
+                add_along(chunk, part, k, inner_up, line)
+            return c
+
+        lax.fori_loop(first, last, one, 0)
+
     def inward_where(runs, chunk):
         @pl.when(runs == 1)
         def _():
             w_take(chunk).wait_recv()
 
-        for part in parts_of(chunk):
-
-            def one(k, c):
-                line = inner_up * (lines - 1 - k) + (1 - inner_up) * k
-                add_along(chunk, part, k, inner_up, line)
-                return c
-
-            lax.fori_loop(0, runs * inner_count, one, 0)
+        inward_span(0, runs * inner_count, chunk)
 
     def inward(end_chunk, mid_chunk):
         end_runs, mid_runs = end_chunk < chunks, mid_chunk >= 0
@@ -897,12 +951,13 @@
     inward(1, -1)
     inward(2, 0)
     wo_first((0,))
-    wo_second(True, False)
+    wo_second(True, False, (0,))
     inward(3, 1)
     wo_first(range(1, WO_PIECES), True, False)
-    wo_first(range(1, WO_PIECES), False, True, at_end)
     outward(0)
+    wo_second(True, False, range(1, WO_PIECES))
     own_chunk(0)
+    wo_rest(2, (0,), True, True, at_end)
     inward(chunks, 2)
     outward(1)
     own_chunk(1)
@@ -932,9 +987,9 @@
 
     for copy in swap_states():
         copy.start()
-    wo_first(range(1, WO_PIECES), False, True, jnp.logical_not(at_end))
-    wo_second(False, True)
-    wo_rest(2, (0,), True, True)
+    wo_first(range(1, WO_PIECES), False, True)
+    wo_second(False, True, (0,))
+    wo_rest(2, (0,), True, False, at_mid)
     wo_rest(2, range(1, WO_PIECES), True, False)
     wo_rest(2, range(1, WO_PIECES), False, True, at_end)
 
@@ -1030,8 +1085,6 @@
         local_num[d] = dot(part.astype(BF16), proj[1], NN)
         local.append((cum_c, peak, jnp.sum(part, axis=-1, keepdims=True)))
 
-    chain_inward()
-    inward(chunks, 4)
     outward(3)
     own_chunk(3)
 
@@ -1057,11 +1110,20 @@
     def _():
         edge(1).start()
 
-    wo_rest(2, range(1, WO_PIECES), False, True, jnp.logical_not(at_end))
+    wo_second(False, True, range(1, WO_PIECES))
+    wo_rest(2, range(WO_PIECES), False, True, jnp.logical_not(at_end))
+    chain_inward()
+
+
+    @pl.when(at_mid)
+    def _():
+        w_take(4).wait_recv()
+
+    inward_span(0, 1 - end_here, 4)
+    chain_outward()
+    inward_span(1, (1 - end_here) * inner_count, 4)
     for away in range(3, lines):
         wo_rest(away, range(1, WO_PIECES))
-    chain_outward()
-    outward(4)
 
     half_rows = rows // 2
 
@@ -1136,11 +1198,13 @@
         own_w = jnp.exp(peak - top)
         num = own_w * local_num[d] + carry_w * dot(query_f.astype(BF16), carry_c[...].astype(BF16), NN)
         den = own_w * den + carry_w * jnp.sum(query_f * carry_n[:, :dk], axis=-1, keepdims=True)
-        result = num / jnp.maximum(jnp.abs(den), jnp.exp(-top))
-        summed = result if d == 0 else summed + result
+        cell = num / jnp.maximum(jnp.abs(den), jnp.exp(-top))
+        summed = cell if d == 0 else summed + cell
     inverse = lax.rsqrt(jnp.mean(summed * summed, axis=-1, keepdims=True) + EPS)
     joined[head, :, :dv] = (summed * inverse * head_gain[...]).astype(BF16)
     share_start(0)
+    outward(4)
+    spread_send()
 
     @pl.when(prior_exists)
     def _():
@@ -1168,7 +1232,25 @@
 
     for line in range(lines):
         for piece in range(WO_PIECES):
-            wo_mate_take(line, piece).wait_recv()
+            if not spread or piece != tail_piece:
+                wo_mate_take(line, piece).wait_recv()
+                continue
+
+            @pl.when(jnp.logical_or(jnp.logical_and(at_mid, line == near_line), jnp.logical_and(at_end, line != near_line)))
+            def _():
+                wo_mate_take(line, piece).wait_recv()
+
+    if spread:
+
+        @pl.when(at_mid)
+        def _():
+            along_row(far_line, 0, 0).wait_recv()
+
+        @pl.when(at_end)
+        def _():
+            along_row(near_line, 0, 1).wait_recv()
+            mate_cut(near_line, 1 - y).wait_recv()
+
     for part in range(2):
         share_wait(part)
 
@@ -1180,7 +1262,16 @@
         total = dot(joined[0], wo_all[0:span_j, span], NN)
         for j in range(1, t):
             total += dot(joined[j], wo_all[j * span_j : (j + 1) * span_j, span], NN)
-        out[:, span] = total.astype(BF16)
+        result[:, span] = total.astype(BF16)
+        put(i).start()
+        return c
+
+    def put(i):
+        span = pl.ds(pl.multiple_of(i * width, width), width)
+        return pltpu.make_async_copy(result.at[:, span], out.at[:, span], out_sem.at[i])
+
+    def put_end(i, c):
+        put(i).wait()
         return c
 
     lax.fori_loop(0, out.shape[1] // width, emit, 0)
@@ -1246,8 +1337,22 @@
             def _():
                 wo_line(line, piece, -1, line).wait_send()
 
-            wo_mate(line, piece).wait_send()
-
+            @pl.when(from_mate(line, piece))
+            def _():
+                wo_mate(line, piece).wait_send()
+
+    if spread:
+
+        @pl.when(at_mid)
+        def _():
+            along_row(z, -inner_way, 1).wait_send()
+            along_row(z - inner_way, inner_way, 0).wait_send()
+
+        @pl.when(at_end)
+        def _():
+            mate_cut(near_line, y).wait_send()
+
+    lax.fori_loop(0, out.shape[1] // width, put_end, 0)
 
 def body(
     n,
@@ -1284,7 +1389,7 @@
         functools.partial(kernel, n, t, dk, dv),
         out_shape=jax.ShapeDtypeStruct((rows, cols), BF16),
         in_specs=[hbm, vmem] + [hbm] * 7 + [vmem] + [smem] * 2 + [vmem] * 3,
-        out_specs=vmem,
+        out_specs=hbm,
         scratch_shapes=[
             pltpu.VMEM((rows, model), BF16),
             pltpu.VMEM((lines, t, rows, part_k), BF16),
@@ -1311,6 +1416,8 @@
             pltpu.VMEM((1, dv), F32),
             pltpu.VMEM((2, rows, dv), F32),
             pltpu.VMEM((t, rows, 2 * dv), BF16),
+            pltpu.VMEM((rows, cols), BF16),
+            dma((cols // 256,)),
             dma((8,)),
             dma((rows // 32,)),
             dma((lines,)),
@@ -1335,6 +1442,8 @@
             dma((lines, WO_PIECES)),
             dma((lines, WO_PIECES)),
             dma((lines, WO_PIECES)),
+            dma((2,)),
+            dma((2,)),
         ],
         compiler_params=pltpu.CompilerParams(
             collective_id=0, has_side_effects=True, vmem_limit_bytes=60 * 1024 * 1024

time: 93.6 us -> 89.5 us (0.956)
  Pallas kernels: 90.8 us -> 87.4 us
    pallas_call x1, Pallas kernels: 90.8 us -> 87.4 us  [body(): pl.pallas_call(functools.partial(kernel, n, t, dk, dv), out_shape=jax.Sha...]
where the time goes in v4:
time: 89.5 us; the launch traced here: 89.3 us
  Pallas kernels  87.4 us (98%)
  local copies, waits for them, and re-layouts  1.87 us (2%)
    pallas_call x1, Pallas kernels, body(): pl.pallas_call(functools.partial(kernel, n, t, dk, dv), out_shape=jax.Sha...  87.4 us
    unnamed x1, local copies, waits for them, and re-layouts  1.87 us

profile of v4, /device:TPU:0, one launch (start us, length us, event | category | flops | bytes accessed | tf_op | source)
XLA Modules:
  0.0 89.3 jit_solution(17133614070637403175)
XLA Ops:
  0.0 87.4 %shard_map.145 = bf16[256,1024]{1,0:T(8,128)(2,1)} custom-call(bf16[256,4096]{1,0:T(8,128)(2,1)} %tokens.1, f32[1,4096]{1,0:T(1,128)} %bitcast.9, bf16[512,128]{1,0:T(8,128)(2,1)} %w_query.1, bf16[512,128]{1,0:T(8,128)(2,1)} %w_key.1, bf16[512,256]{1,0:T(8,128)(2,1)} %w_value.1, bf16[512,256]{1,0:T(8,128)(2,1)} %w_conv_b.1, bf16[512,256]{1,0:T(8,128)(2,1)} %w_conv_c.1, ...), custom_call_target="tpu_custom_call" | custom-call | tf_op jit(solution)/shard_map/pallas_call | solution.py:1388
  87.4 1.9 %copy.17 = bf16[256,1024]{1,0:T(8,128)(2,1)} copy(bf16[256,1024]{1,0:T(8,128)(2,1)} %shard_map.145) | data formatting | bytes 1048576

commit v5 on v4

--- a/solution.py
+++ b/solution.py
@@ -517,6 +517,7 @@
     local_num,
     joined,
     result,
+    out_acc,
     out_sem,
     own_sem,
     tok_sem,
@@ -536,7 +537,6 @@
     ed_rs,
     j_ss,
     j_rs,
-    jp_ss,
     jp_rs,
     oz_ss,
     oz_rs,
@@ -630,27 +630,25 @@
 
     def token_send(line):
         return pltpu.make_async_remote_copy(
-            nbuf.at[line, head], tall.at[z, head], tk_ss.at[line], tk_rs.at[z], device_id={"sp": at_line(line)}
+            nbuf.at[line, head], tall.at[z, head], tk_ss.at[0], tk_rs.at[z], device_id={"sp": at_line(line)}
         )
 
     def token_take(line):
         return pltpu.make_async_remote_copy(
-            nbuf.at[line, head], tall.at[line, head], tk_ss.at[line], tk_rs.at[line], device_id={"sp": at_line(line)}
+            nbuf.at[line, head], tall.at[line, head], tk_ss.at[0], tk_rs.at[line], device_id={"sp": at_line(line)}
         )
 
     def token_pass(line, way):
         quarter = (head, head, x_mate)[way]
         there = tall.at[line, quarter]
+        sem = lines if way != 1 else line
         return pltpu.make_async_remote_copy(
-            there, there, tf_ss.at[way, line], tf_rs.at[way, line], device_id={"tp": (core_mate, x_mate, core_mate)[way]}
-        )
-
-    def token_get(line, way):
-        quarter = (core_mate, x_mate, far_mate)[way]
-        there = tall.at[line, quarter]
-        return pltpu.make_async_remote_copy(
-            there, there, tf_ss.at[way, line], tf_rs.at[way, line], device_id={"tp": (core_mate, x_mate, core_mate)[way]}
-        )
+            there, there, tf_ss.at[0], tf_rs.at[sem], device_id={"tp": (core_mate, x_mate, core_mate)[way]}
+        )
+
+    def token_get(line):
+        there = tall.at[line, x_mate]
+        return pltpu.make_async_remote_copy(there, there, tf_ss.at[0], tf_rs.at[line], device_id={"tp": x_mate})
 
     def send_tokens(k, c):
         _, line = pick(k, False)
@@ -661,11 +659,11 @@
 
     def w_send(chunk):
         there = wbuf.at[chunk, mine, :]
-        return pltpu.make_async_remote_copy(there, there, w_ss.at[chunk], w_rs.at[chunk], device_id={"sp": mate})
+        return pltpu.make_async_remote_copy(there, there, w_ss.at[0], w_rs.at[chunk], device_id={"sp": mate})
 
     def w_take(chunk):
         there = wbuf.at[chunk, pl.ds(pl.multiple_of((1 - y) * depth, depth), depth), :]
-        return pltpu.make_async_remote_copy(there, there, w_ss.at[chunk], w_rs.at[chunk], device_id={"sp": mate})
+        return pltpu.make_async_remote_copy(there, there, w_ss.at[0], w_rs.at[chunk], device_id={"sp": mate})
 
     for load in loads:
         load.wait()
@@ -680,19 +678,19 @@
     def wo_line(line, piece, way, sem):
         there = wo_rows(at_line(line), piece)
         return pltpu.make_async_remote_copy(
-            there, there, oz_ss.at[sem, piece], oz_rs.at[line, piece], device_id={"sp": at_line(z + way)}
+            there, there, oz_ss.at[0], oz_rs.at[line, piece], device_id={"sp": at_line(z + way)}
         )
 
     def wo_mate(line, piece):
         there = wo_rows(at_line(line), piece)
         return pltpu.make_async_remote_copy(
-            there, there, oy_ss.at[line, piece], oy_rs.at[line, piece], device_id={"sp": mate}
+            there, there, oy_ss.at[0], oy_rs.at[line, piece], device_id={"sp": mate}
         )
 
     def wo_mate_take(line, piece):
         there = wo_rows(PAIR * line + 1 - y, piece)
         return pltpu.make_async_remote_copy(
-            there, there, oy_ss.at[line, piece], oy_rs.at[line, piece], device_id={"sp": mate}
+            there, there, oy_ss.at[0], oy_rs.at[line, piece], device_id={"sp": mate}
         )
 
     def wo_own(way, wanted):
@@ -756,7 +754,7 @@
     def mate_cut(line, row):
         there = cut_rows(PAIR * line + row, 1, 2)
         return pltpu.make_async_remote_copy(
-            there, there, oy_ss.at[line, tail_piece], oy_rs.at[line, tail_piece], device_id={"sp": mate}
+            there, there, oy_ss.at[0], oy_rs.at[line, tail_piece], device_id={"sp": mate}
         )
 
     def along_row(line, way, kind):
@@ -828,21 +826,16 @@
 
     def relay_across(k, c):
         _, line = pick(k, True)
-        token_get(line, 1).wait_recv()
+        token_get(line).wait_recv()
         token_pass(line, 2).start()
-        return c
-
-    def tokens_ready(k, c):
-        _, line = pick(k, True)
-        token_get(line, 0).wait_recv()
-        token_get(line, 2).wait_recv()
         return c
 
     lax.fori_loop(0, lines - 1, relay_direct, 0)
     wo_outward()
     wo_inward(False)
     lax.fori_loop(0, lines - 1, relay_across, 0)
-    lax.fori_loop(0, lines - 1, tokens_ready, 0)
+    both = tall.at[pl.ds(0, lines - 1), pl.ds(0, 2)]
+    pltpu.make_async_remote_copy(both, both, tf_ss.at[0], tf_rs.at[lines], device_id={"tp": core_mate}).wait_recv()
     def parts_of(chunk):
         if isinstance(chunk, int) and chunk == chunks - 1:
             return ((0, rows // 2, chunk), (rows // 2, rows // 2, chunks))
@@ -855,7 +848,7 @@
         return pltpu.make_async_remote_copy(
             sbuf.at[chunk, k, pl.ds(first, count)],
             rbuf.at[chunk, slot, pl.ds(first, count)],
-            rs_ss.at[sem, k],
+            rs_ss.at[0],
             rs_rs.at[sem, slot],
             device_id={"sp": at_line(z + 2 * up - 1)},
         )
@@ -865,7 +858,7 @@
         return pltpu.make_async_remote_copy(
             sbuf.at[chunk, 0, pl.ds(first, count)],
             rbuf.at[chunk, slot, pl.ds(first, count)],
-            rs_ss.at[sem, 0],
+            rs_ss.at[0],
             rs_rs.at[sem, slot],
             device_id={"sp": me},
         )
@@ -1138,13 +1131,13 @@
     def share(part, way, source):
         slot = joined_part(part, source, way)
         return pltpu.make_async_remote_copy(
-            slot, slot, j_ss.at[part, way], j_rs.at[part, way], device_id={"tp": others[way]}
+            slot, slot, j_ss.at[0], j_rs.at[part, way], device_id={"tp": others[way]}
         )
 
     def share_pass(part, way, source):
         slot = joined_part(part, source, way)
         return pltpu.make_async_remote_copy(
-            slot, slot, jp_ss.at[part, way - 1], jp_rs.at[part, way - 1], device_id={"tp": core_mate}
+            slot, slot, j_ss.at[0], jp_rs.at[part, way - 1], device_id={"tp": core_mate}
         )
 
     def share_start(part):
@@ -1160,12 +1153,6 @@
         share(part, 0, core_mate).wait_recv()
         for way in (1, 2):
             share_pass(part, way, others[3 - way]).wait_recv()
-
-    def share_end(part):
-        for way in range(3):
-            share(part, way, head).wait_send()
-        for way in (1, 2):
-            share_pass(part, way, others[way]).wait_send()
 
     summed = None
     query_f = proj[0, :, :dk].astype(F32) * scale
@@ -1251,18 +1238,26 @@
             along_row(near_line, 0, 1).wait_recv()
             mate_cut(near_line, 1 - y).wait_recv()
 
-    for part in range(2):
-        share_wait(part)
-
-    span_j = 2 * dv
-    width = 256
+    share_wait(0)
+    width = 512
+
+    def columns_of(part, i):
+        span = pl.ds(pl.multiple_of(i * width, width), width)
+        total = None
+        for j in range(t):
+            first = (2 * j + part) * dv
+            term = dot(joined[j, :, part * dv : (part + 1) * dv], wo_all[first : first + dv, span], NN)
+            total = term if j == 0 else total + term
+        return span, total
+
+    def emit_cell(i, c):
+        span, total = columns_of(0, i)
+        out_acc[:, span] = total
+        return c
 
     def emit(i, c):
-        span = pl.ds(pl.multiple_of(i * width, width), width)
-        total = dot(joined[0], wo_all[0:span_j, span], NN)
-        for j in range(1, t):
-            total += dot(joined[j], wo_all[j * span_j : (j + 1) * span_j, span], NN)
-        result[:, span] = total.astype(BF16)
+        span, total = columns_of(1, i)
+        result[:, span] = (out_acc[:, span] + total).astype(BF16)
         put(i).start()
         return c
 
@@ -1274,25 +1269,42 @@
         put(i).wait()
         return c
 
+    lax.fori_loop(0, out.shape[1] // width, emit_cell, 0)
+    share_wait(1)
     lax.fori_loop(0, out.shape[1] // width, emit, 0)
 
-    def token_end(k, c):
-        _, line = pick(k, False)
-        token_send(line).wait_send()
-        for way in range(3):
-            token_pass(line, way).wait_send()
-        inner = jnp.clip(inner_count - k, 0, 1)
-        up = inner * inner_up + (1 - inner) * (1 - inner_up)
-        step = inner * k + (1 - inner) * (k - inner_count)
-        line = up * (lines - 1 - step) + (1 - up) * step
-        for chunk in range(chunks):
-            for part in parts_of(chunk):
-                hop(chunk, part, k, up, line).wait_send()
-        return c
-
-    lax.fori_loop(0, lines - 1, token_end, 0)
-    for chunk in range(chunks):
-        w_send(chunk).wait_send()
+    def sent(ref, sem):
+        pltpu.make_async_remote_copy(ref, ref, sem.at[0], w_rs.at[0], device_id={"sp": mate}).wait_send()
+
+    sent(nbuf.at[pl.ds(0, lines - 1), 0], tk_ss)
+    sent(tall.at[pl.ds(0, lines - 1), pl.ds(0, 3)], tf_ss)
+    sent(wbuf.at[:, mine, :], w_ss)
+    sent(sbuf, rs_ss)
+    sent(joined.at[pl.ds(0, 3)], j_ss)
+
+    @pl.when(at_end)
+    def _():
+        sent(wo_all.at[pl.ds(0, depth_o)], oz_ss)
+
+    @pl.when(at_mid)
+    def _():
+        sent(wo_all.at[pl.ds(0, (lines + 1) * depth_o)], oz_ss)
+
+    if spread:
+
+        @pl.when(at_end)
+        def _():
+            sent(wo_all.at[pl.ds(0, lines * depth_o - tall_o + tall_o // 2)], oy_ss)
+
+        @pl.when(at_mid)
+        def _():
+            sent(wo_all.at[pl.ds(0, lines * depth_o - tall_o)], oy_ss)
+            along_row(z, -inner_way, 1).wait_send()
+            along_row(z - inner_way, inner_way, 0).wait_send()
+
+    else:
+        sent(wo_all.at[pl.ds(0, lines * depth_o)], oy_ss)
+
     for copy in swap_states():
         copy.wait_send()
 
@@ -1315,42 +1327,6 @@
     def _():
         edge(1).wait_send()
 
-    for part in range(2):
-        share_end(part)
-    for piece in range(WO_PIECES):
-
-        @pl.when(has_up)
-        def _():
-            wo_line(z, piece, 1, lines + 1).wait_send()
-
-        @pl.when(has_down)
-        def _():
-            wo_line(z, piece, -1, lines).wait_send()
-
-        for line in range(lines):
-
-            @pl.when(jnp.logical_and(z > line, has_up))
-            def _():
-                wo_line(line, piece, 1, line).wait_send()
-
-            @pl.when(jnp.logical_and(z < line, has_down))
-            def _():
-                wo_line(line, piece, -1, line).wait_send()
-
-            @pl.when(from_mate(line, piece))
-            def _():
-                wo_mate(line, piece).wait_send()
-
-    if spread:
-
-        @pl.when(at_mid)
-        def _():
-            along_row(z, -inner_way, 1).wait_send()
-            along_row(z - inner_way, inner_way, 0).wait_send()
-
-        @pl.when(at_end)
-        def _():
-            mate_cut(near_line, y).wait_send()
 
     lax.fori_loop(0, out.shape[1] // width, put_end, 0)
 
@@ -1417,16 +1393,17 @@
             pltpu.VMEM((2, rows, dv), F32),
             pltpu.VMEM((t, rows, 2 * dv), BF16),
             pltpu.VMEM((rows, cols), BF16),
+            pltpu.VMEM((rows, cols), F32),
             dma((cols // 256,)),
             dma((8,)),
             dma((rows // 32,)),
+            dma((1,)),
             dma((lines,)),
-            dma((lines,)),
-            dma((3, lines)),
-            dma((3, lines)),
+            dma((1,)),
+            dma((lines + 1,)),
+            dma((1,)),
             dma((chunks,)),
-            dma((chunks,)),
-            dma((chunks + 1, lines - 1)),
+            dma((1,)),
             dma((chunks + 1, lines + 1)),
             dma((3,)),
             dma((3,)),
@@ -1434,13 +1411,12 @@
             dma((3,)),
             dma((2,)),
             dma((2,)),
-            dma((2, 3)),
+            dma((1,)),
             dma((2, 3)),
             dma((2, 2)),
-            dma((2, 2)),
-            dma((lines + 2, WO_PIECES)),
+            dma((1,)),
             dma((lines, WO_PIECES)),
-            dma((lines, WO_PIECES)),
+            dma((1,)),
             dma((lines, WO_PIECES)),
             dma((2,)),
             dma((2,)),

time: 89.5 us -> 88 us (0.983)
  Pallas kernels: 87.4 us -> 85.9 us
    pallas_call x1, Pallas kernels: 87.4 us -> 85.9 us  [body(): pl.pallas_call(functools.partial(kernel, n, t, dk, dv), out_shape=jax.Sha...]
where the time goes in v5:
time: 88 us; the launch traced here: 87.8 us
  Pallas kernels  85.9 us (98%)
  local copies, waits for them, and re-layouts  1.87 us (2%)
    pallas_call x1, Pallas kernels, body(): pl.pallas_call(functools.partial(kernel, n, t, dk, dv), out_shape=jax.Sha...  85.9 us
    unnamed x1, local copies, waits for them, and re-layouts  1.87 us

profile of v5, /device:TPU:0, one launch (start us, length us, event | category | flops | bytes accessed | tf_op | source)
XLA Modules:
  0.0 87.8 jit_solution(3392914158436871600)
XLA Ops:
  0.0 85.9 %shard_map.145 = bf16[256,1024]{1,0:T(8,128)(2,1)} custom-call(bf16[256,4096]{1,0:T(8,128)(2,1)} %tokens.1, f32[1,4096]{1,0:T(1,128)} %bitcast.9, bf16[512,128]{1,0:T(8,128)(2,1)} %w_query.1, bf16[512,128]{1,0:T(8,128)(2,1)} %w_key.1, bf16[512,256]{1,0:T(8,128)(2,1)} %w_value.1, bf16[512,256]{1,0:T(8,128)(2,1)} %w_conv_b.1, bf16[512,256]{1,0:T(8,128)(2,1)} %w_conv_c.1, ...), custom_call_target="tpu_custom_call" | custom-call | tf_op jit(solution)/shard_map/pallas_call | solution.py:1364
  85.9 1.9 %copy.17 = bf16[256,1024]{1,0:T(8,128)(2,1)} copy(bf16[256,1024]{1,0:T(8,128)(2,1)} %shard_map.145) | data formatting | bytes 1048576

commit v6 on v5

--- a/solution.py
+++ b/solution.py
@@ -563,6 +563,21 @@
     def at_line(line):
         return PAIR * line + y
 
+    edge_in[...] = jnp.zeros_like(edge_in)
+
+    barrier = pltpu.get_barrier_semaphore()
+
+    def greet_sp(o, c):
+        pl.semaphore_signal(barrier, inc=1, device_id={"sp": lax.rem(me + o, n)})
+        return c
+
+    def greet_tp(o, c):
+        pl.semaphore_signal(barrier, inc=1, device_id={"tp": lax.rem(head + o, t)})
+        return c
+
+    lax.fori_loop(1, n, greet_sp, 0)
+    lax.fori_loop(1, t, greet_tp, 0)
+
     rows_at_once = 32
 
     def load_rows(i):
@@ -585,21 +600,6 @@
     loads.append(pltpu.make_async_copy(w_out, spot, own_sem.at[1 + len(loads)]))
     for load in loads:
         load.start()
-
-    edge_in[...] = jnp.zeros_like(edge_in)
-
-    barrier = pltpu.get_barrier_semaphore()
-
-    def greet_sp(o, c):
-        pl.semaphore_signal(barrier, inc=1, device_id={"sp": lax.rem(me + o, n)})
-        return c
-
-    def greet_tp(o, c):
-        pl.semaphore_signal(barrier, inc=1, device_id={"tp": lax.rem(head + o, t)})
-        return c
-
-    lax.fori_loop(1, n, greet_sp, 0)
-    lax.fori_loop(1, t, greet_tp, 0)
 
     def norm_rows(i, c):
         load_rows(i).wait()
@@ -830,9 +830,9 @@
         token_pass(line, 2).start()
         return c
 
+    wo_inward(False)
     lax.fori_loop(0, lines - 1, relay_direct, 0)
     wo_outward()
-    wo_inward(False)
     lax.fori_loop(0, lines - 1, relay_across, 0)
     both = tall.at[pl.ds(0, lines - 1), pl.ds(0, 2)]
     pltpu.make_async_remote_copy(both, both, tf_ss.at[0], tf_rs.at[lines], device_id={"tp": core_mate}).wait_recv()

time: 88 us -> 87.1 us (0.990)
  Pallas kernels: 85.9 us -> 85 us
where the time goes in v6:
time: 87.1 us; the launch traced here: 86.9 us
  Pallas kernels  85 us (98%)
  local copies, waits for them, and re-layouts  1.87 us (2%)
    pallas_call x1, Pallas kernels, body(): pl.pallas_call(functools.partial(kernel, n, t, dk, dv), out_shape=jax.Sha...  85 us
    unnamed x1, local copies, waits for them, and re-layouts  1.87 us

profile of v6, /device:TPU:0, one launch (start us, length us, event | category | flops | bytes accessed | tf_op | source)
XLA Modules:
  0.0 86.9 jit_solution(11564963623288859791)
XLA Ops:
  0.0 85.0 %shard_map.145 = bf16[256,1024]{1,0:T(8,128)(2,1)} custom-call(bf16[256,4096]{1,0:T(8,128)(2,1)} %tokens.1, f32[1,4096]{1,0:T(1,128)} %bitcast.9, bf16[512,128]{1,0:T(8,128)(2,1)} %w_query.1, bf16[512,128]{1,0:T(8,128)(2,1)} %w_key.1, bf16[512,256]{1,0:T(8,128)(2,1)} %w_value.1, bf16[512,256]{1,0:T(8,128)(2,1)} %w_conv_b.1, bf16[512,256]{1,0:T(8,128)(2,1)} %w_conv_c.1, ...), custom_call_target="tpu_custom_call" | custom-call | tf_op jit(solution)/shard_map/pallas_call | solution.py:1364
  85.0 1.9 %copy.17 = bf16[256,1024]{1,0:T(8,128)(2,1)} copy(bf16[256,1024]{1,0:T(8,128)(2,1)} %shard_map.145) | data formatting | bytes 1048576
